TPU v7x, 32 devices: a whole 2x2x4 slice. The times are simulated.
32 devices in a mesh: gr: 2 (over x), fs: 8 (over z, y), tp: 2 (over core).
Axes of the slice: x: 2, y: 2, z: 4, core: 2. Of those that a mesh axis runs over, the one named last changes fastest.
Arguments:
- prompt: bfloat16 [3072, 2048], P(('gr', 'fs', 'tp')), may hold values from -6 to 6
- norm_first: float32 [2048], P(('gr', 'fs')), may hold values from 0.1 to 1.9
- gate_first: float32 [2048, 5632], P(('gr', 'fs'), 'tp'), may hold values from -6 to 6
- up_first: float32 [2048, 5632], P(('gr', 'fs'), 'tp'), may hold values from -6 to 6
- down_first: float32 [2048, 5632], P(('gr', 'fs'), 'tp'), may hold values from -6 to 6
- norm_second: float32 [2048], P(('gr', 'fs')), may hold values from 0.1 to 1.9
- gate_second: float32 [2048, 5632], P(('gr', 'fs'), 'tp'), may hold values from -6 to 6
- up_second: float32 [2048, 5632], P(('gr', 'fs'), 'tp'), may hold values from -6 to 6
- down_second: float32 [2048, 5632], P(('gr', 'fs'), 'tp'), may hold values from -6 to 6
Outputs:
- served_gate_first: bfloat16 [2048, 5632], P(None, 'fs')
- served_up_first: bfloat16 [2048, 5632], P(None, 'fs')
- served_down_first: bfloat16 [2048, 5632], P(None, 'fs')
- served_gate_second: bfloat16 [2048, 5632], P(None, 'fs')
- served_up_second: bfloat16 [2048, 5632], P(None, 'fs')
- served_down_second: bfloat16 [2048, 5632], P(None, 'fs')
- result: bfloat16 [3072, 2048], P(('gr', 'fs', 'tp'))
All inputs are finite; a program needn't handle non-finite values.
Results may differ from a plain program's by a relative error of at most 0.015.
Values may be sent and summed in bfloat16 or wider, within the bound.
A program may use at most 128 MiB of HBM per device.

v0:
```python
import functools

import jax
import jax.numpy as jnp
from jax import lax
from jax.experimental import pallas as pl
from jax.experimental.pallas import tpu as pltpu
from jax.sharding import PartitionSpec as P

EPS = 1e-06
MESH = pl.DeviceIdType.MESH


def fold_rows(gain, weight):
    return (gain[:, None] * weight).astype(jnp.bfloat16)


def relayout_kernel(sizes, pieces, *refs):
    gr, fs, tp = sizes
    mats, blocks, rows, _ = pieces.shape
    outs = refs[:mats]
    first_send, first_recv, gr_send, gr_recv, tp_send, tp_recv = refs[mats:]
    g, f, t = lax.axis_index("gr"), lax.axis_index("fs"), lax.axis_index("tp")
    sub = rows // tp

    def rows_of(m, from_gr, from_fs, core):
        start = pl.multiple_of((from_gr * fs + from_fs) * rows + core * sub, sub)
        return outs[m].at[pl.ds(start, sub)]

    def remote(src, dst, send_sem, recv_sem, device):
        return pltpu.make_async_remote_copy(
            src_ref=src,
            dst_ref=dst,
            send_sem=send_sem,
            recv_sem=recv_sem,
            device_id=device,
            device_id_type=MESH,
        )

    def first_copies(step, act):
        slot = (step + f) % blocks
        block = t * blocks + slot
        for core in range(tp):
            mine = jnp.logical_and(block == f, t == core)
            for m in range(mats):
                source = pieces.at[m, slot, pl.ds(core * sub, sub)]
                target = rows_of(m, g, f, core)
                act(
                    mine,
                    lambda: pltpu.make_async_copy(source, target, first_recv.at[m, f]),
                    lambda: remote(
                        source,
                        target,
                        first_send.at[m, slot, core],
                        first_recv.at[m, f],
                        (g, block, core),
                    ),
                )

    def start(mine, local, far):
        @pl.when(mine)
        def _():
            local().start()

        @pl.when(jnp.logical_not(mine))
        def _():
            far().start()

    def finish(mine, local, far):
        @pl.when(jnp.logical_not(mine))
        def _():
            far().wait_send()

    def origin(step):
        return ((f // blocks + step % tp) % tp) * blocks + (f + blocks - step // tp) % blocks

    def to_peers(m, ref):
        for hop in range(1, tp):
            remote(ref, ref, tp_send.at[m], tp_recv.at[m], (g, f, (t + hop) % tp)).start()

    def send_first(step, carry):
        first_copies(step, start)
        return carry

    def pass_on(step, carry):
        source = origin(step)
        for m in range(mats):
            ref = rows_of(m, g, source, t)
            pltpu.make_async_copy(ref, ref, first_recv.at[m, source]).wait()
            for hop in range(1, gr):
                remote(
                    ref,
                    ref,
                    gr_send.at[m],
                    gr_recv.at[m, hop - 1, source],
                    ((g + hop) % gr, f, t),
                ).start()
            to_peers(m, ref)
        return carry

    def pass_on_far(step, carry):
        source = origin(step)
        for m in range(mats):
            for hop in range(1, gr):
                ref = rows_of(m, (g + gr - hop) % gr, source, t)
                pltpu.make_async_copy(ref, ref, gr_recv.at[m, hop - 1, source]).wait()
                to_peers(m, ref)
        return carry

    def finish_first(step, carry):
        first_copies(step, finish)
        return carry

    lax.fori_loop(0, blocks, send_first, 0)
    lax.fori_loop(0, fs, pass_on, 0)
    lax.fori_loop(0, fs, pass_on_far, 0)
    lax.fori_loop(0, blocks, finish_first, 0)

    def wait_rows(m, count, sem):
        if count:
            ref = outs[m].at[pl.ds(0, count)]
            pltpu.make_async_copy(ref, ref, sem).wait()

    for m in range(mats):
        wait_rows(m, fs * sub * (gr - 1), gr_send.at[m])
        wait_rows(m, gr * fs * sub * (tp - 1), tp_send.at[m])
        wait_rows(m, gr * fs * sub * (tp - 1), tp_recv.at[m])


def relayout(pieces, sizes):
    gr, fs, tp = sizes
    mats, blocks, rows, width = pieces.shape
    total = gr * fs * rows
    served = jax.ShapeDtypeStruct((total, width), pieces.dtype)
    return pl.pallas_call(
        functools.partial(relayout_kernel, sizes),
        out_shape=[served] * mats,
        in_specs=[pl.BlockSpec(memory_space=pltpu.VMEM)],
        out_specs=[pl.BlockSpec(memory_space=pl.ANY)] * mats,
        scratch_shapes=[
            pltpu.SemaphoreType.DMA((mats, blocks, tp)),
            pltpu.SemaphoreType.DMA((mats, fs)),
            pltpu.SemaphoreType.DMA((mats,)),
            pltpu.SemaphoreType.DMA((mats, max(gr - 1, 1), fs)),
            pltpu.SemaphoreType.DMA((mats,)),
            pltpu.SemaphoreType.DMA((mats,)),
        ],
        compiler_params=pltpu.CompilerParams(has_side_effects=True),
        cost_estimate=pl.CostEstimate(
            flops=0, bytes_accessed=mats * total * width * 24, transcendentals=0
        ),
        name="relayout",
    )(pieces)


def cut(matrices, blocks):
    rows, columns = matrices[0].shape
    return jnp.stack(
        [m.reshape(rows, blocks, columns // blocks).transpose(1, 0, 2) for m in matrices]
    )


def normed_tokens(resid_f):
    return (
        resid_f * lax.rsqrt(jnp.mean(resid_f * resid_f, axis=-1, keepdims=True) + EPS)
    ).astype(jnp.bfloat16)


def partial_branch(tokens_in, weights):
    gate_weight, up_weight, down_weight = weights
    in_scale = gate_weight.shape[0] ** (-0.5)
    out_scale = (down_weight.shape[1] * lax.axis_size("fs")) ** (-0.5)
    gate_pre = jnp.dot(tokens_in, gate_weight, preferred_element_type=jnp.float32) * in_scale
    up_pre = jnp.dot(tokens_in, up_weight, preferred_element_type=jnp.float32) * in_scale
    hidden = (jax.nn.silu(gate_pre) * up_pre).astype(jnp.bfloat16)
    return (
        lax.dot_general(
            hidden, down_weight, (((1,), (1,)), ((), ())), preferred_element_type=jnp.float32
        )
        * out_scale
    ).astype(jnp.bfloat16)


def gather_tokens(normed):
    return lax.all_gather(normed, "fs", axis=0, tiled=True)


def scatter_sum(partial):
    return lax.psum_scatter(partial, "fs", scatter_dimension=0, tiled=True)


def on_device(
    prompt,
    norm_first,
    gate_first,
    up_first,
    down_first,
    norm_second,
    gate_second,
    up_second,
    down_second,
):
    sizes = tuple(lax.axis_size(axis) for axis in ("gr", "fs", "tp"))
    blocks = sizes[1] // sizes[2]
    prompt_f = prompt.astype(jnp.float32)
    tokens_first = gather_tokens(normed_tokens(prompt_f))
    pieces_first = cut(
        [
            fold_rows(norm_first, gate_first),
            fold_rows(norm_first, up_first),
            down_first.astype(jnp.bfloat16),
        ],
        blocks,
    )
    served_first = relayout(pieces_first, sizes)
    partial_first = partial_branch(tokens_first, served_first)
    gate_second, up_second, partial_first = lax.optimization_barrier(
        (gate_second, up_second, partial_first)
    )
    served_in = relayout(
        cut([fold_rows(norm_second, gate_second), fold_rows(norm_second, up_second)], blocks),
        sizes,
    )
    branch_first, *served_in = lax.optimization_barrier((scatter_sum(partial_first), *served_in))
    middle = (prompt_f + 0.5 * branch_first.astype(jnp.float32)).astype(jnp.bfloat16)
    middle_f = middle.astype(jnp.float32)
    normed, down_second = lax.optimization_barrier((normed_tokens(middle_f), down_second))
    tokens_second = gather_tokens(normed)
    served_out = relayout(cut([down_second.astype(jnp.bfloat16)], blocks), sizes)
    served_second = (*served_in, *served_out)
    branch_second = scatter_sum(partial_branch(tokens_second, served_second)).astype(jnp.float32)
    result = (middle_f + 0.5 * branch_second).astype(jnp.bfloat16)
    return (*served_first, *served_second, result)


def solution(mesh):
    in_specs = (
        P(("gr", "fs", "tp"), None),
        P(("gr", "fs")),
        P(("gr", "fs"), "tp"),
        P(("gr", "fs"), "tp"),
        P(("gr", "fs"), "tp"),
        P(("gr", "fs")),
        P(("gr", "fs"), "tp"),
        P(("gr", "fs"), "tp"),
        P(("gr", "fs"), "tp"),
    )
    out_specs = (
        P(None, "fs"),
        P(None, "fs"),
        P(None, "fs"),
        P(None, "fs"),
        P(None, "fs"),
        P(None, "fs"),
        P(("gr", "fs", "tp"), None),
    )
    return jax.shard_map(
        on_device, mesh=mesh, in_specs=in_specs, out_specs=out_specs, check_vma=False
    )
```

profile of v0, /device:TPU:0, one launch (start us, length us, event | category | flops | bytes accessed | tf_op | source)
XLA Modules:
  0.0 408.8 jit_solution(11439917173379199224)
XLA Ops:
  7.2 1.3 fusion
  8.5 1.9 fusion.1
  12.9 1.8 copy.24
  14.7 1.3 multiply_convert_fusion.7
  16.1 1.5 copy.25
  17.5 1.4 copy.23
  18.9 1.7 pad_maximum_fusion.pieces
  20.6 100.5 %relayout.3 = (bf16[2048,704]{1,0:T(8,128)(2,1)}, bf16[2048,704]{1,0:T(8,128)(2,1)}, bf16[2048,704]{1,0:T(8,128)(2,1)}) custom-call(bf16[3,4,128,704]{3,2,1,0:T(8,128)(2,1)} %pad_maximum_fusion.pieces), custom_call_target="tpu_custom_call" | custom-call | bytes 103809024 | tf_op jit(solution)/shard_map/relayout/pallas_call | solution.py:135
  121.2 6.8 %fusion.10 = f32[768,704]{0,1:T(8,128)} fusion(bf16[768,2048]{1,0:T(8,128)(2,1)} %all-gather.3.cloned.1.call-done, bf16[2048,704]{1,0:T(8,128)(2,1)} %get-tuple-element.40), kind=kOutput, calls=%fused_computation.28 | convolution fusion | flops 2214592512 | bytes 8192000 | tf_op jit(solution)/shard_map/dot_general | solution.py:173
  128.0 11.5 %multiply_convert_fusion.1 = bf16[768,2048]{1,0:T(8,128)(2,1)} fusion(bf16[2048,704]{1,0:T(8,128)(2,1)S(1)} %copy-done.3, f32[768,704]{0,1:T(8,128)} %fusion.10, bf16[768,2048]{1,0:T(8,128)(2,1)} %all-gather.3.cloned.1.call-done, bf16[2048,704]{1,0:T(8,128)(2,1)} %get-tuple-element.41), kind=kOutput, calls=%fused_computation.1 | convolution fusion | flops 4436656128 | bytes 14221312 | tf_op jit(solution)/shard_map/dot_general | solution.py:177
  141.3 1.8 copy.30
  143.1 1.3 multiply_convert_fusion.5
  144.4 1.4 copy.31
  145.8 1.4 copy.29
  147.2 1.3 pad_maximum_fusion.1.pieces
  148.5 70.0 %relayout.4 = (bf16[2048,704]{1,0:T(8,128)(2,1)}, bf16[2048,704]{1,0:T(8,128)(2,1)}) custom-call(bf16[2,4,128,704]{3,2,1,0:T(8,128)(2,1)} %pad_maximum_fusion.1.pieces), custom_call_target="tpu_custom_call" | custom-call | bytes 69206016 | tf_op jit(solution)/shard_map/relayout/pallas_call | solution.py:135
  218.5 18.3 %reduce-scatter.3.cloned.1.call-done = bf16[96,2048]{1,0:T(8,128)(2,1)} async-done(((bf16[768,2048]{1,0:T(8,128)(2,1)}), bf16[96,2048]{1,0:T(8,128)(2,1)}) %reduce-scatter.3.cloned.1.call-update) | async-done | bytes 393232 | tf_op jit(solution)/shard_map/reduce_scatter | solution.py:189
  236.8 1.2 fusion.3
  238.1 1.9 fusion.4
  240.4 1.2 copy.33
  241.6 45.4 %relayout.5 = bf16[2048,704]{1,0:T(8,128)(2,1)} custom-call(bf16[1,4,128,704]{3,2,1,0:T(8,128)(2,1)} %bitcast.39), custom_call_target="tpu_custom_call" | custom-call | bytes 34603008 | tf_op jit(solution)/shard_map/relayout/pallas_call | solution.py:135
  287.0 22.0 %all-gather.5.cloned.1.call-done = bf16[768,2048]{1,0:T(8,128)(2,1)} async-done(((bf16[96,2048]{1,0:T(8,128)(2,1)}), bf16[768,2048]{1,0:T(8,128)(2,1)}) %all-gather.5.cloned.1.call-update) | async-done | bytes 3145744 | tf_op jit(solution)/shard_map/all_gather | solution.py:185
  309.0 6.6 %fusion.11 = f32[768,704]{0,1:T(8,128)} fusion(bf16[768,2048]{1,0:T(8,128)(2,1)} %all-gather.5.cloned.1.call-done, bf16[2048,704]{1,0:T(8,128)(2,1)} %get-tuple-element.43), kind=kOutput, calls=%fused_computation.29 | convolution fusion | flops 2214592512 | bytes 8192000 | tf_op jit(solution)/shard_map/dot_general | solution.py:173
  315.7 11.5 %multiply_convert_fusion = bf16[768,2048]{1,0:T(8,128)(2,1)} fusion(bf16[2048,704]{1,0:T(8,128)(2,1)S(1)} %copy-done, f32[768,704]{0,1:T(8,128)} %fusion.11, bf16[768,2048]{1,0:T(8,128)(2,1)} %all-gather.5.cloned.1.call-done, bf16[2048,704]{1,0:T(8,128)(2,1)} %get-tuple-element.44), kind=kOutput, calls=%fused_computation | convolution fusion | flops 4436656128 | bytes 14221312 | tf_op jit(solution)/shard_map/dot_general | solution.py:177
  327.2 4.6 %copy.35 = bf16[2048,704]{0,1:T(8,128)(2,1)} copy(bf16[2048,704]{1,0:T(8,128)(2,1)} %get-tuple-element.41) | data formatting | bytes 5767168
  331.8 4.6 %copy.36 = bf16[2048,704]{0,1:T(8,128)(2,1)} copy(bf16[2048,704]{1,0:T(8,128)(2,1)} %get-tuple-element.42) | data formatting | bytes 5767168
  336.4 4.6 %copy.34 = bf16[2048,704]{0,1:T(8,128)(2,1)} copy(bf16[2048,704]{1,0:T(8,128)(2,1)} %get-tuple-element.40) | data formatting | bytes 5767168
  340.9 4.6 %copy.37 = bf16[2048,704]{0,1:T(8,128)(2,1)} copy(bf16[2048,704]{1,0:T(8,128)(2,1)} %get-tuple-element.43) | data formatting | bytes 5767168
  345.5 4.6 %copy.38 = bf16[2048,704]{0,1:T(8,128)(2,1)} copy(bf16[2048,704]{1,0:T(8,128)(2,1)} %get-tuple-element.44) | data formatting | bytes 5767168
  350.1 2.7 copy.39
  352.8 47.4 %reduce-scatter.5.cloned.1.call-done = bf16[96,2048]{1,0:T(8,128)(2,1)} async-done(((bf16[768,2048]{1,0:T(8,128)(2,1)}), bf16[96,2048]{1,0:T(8,128)(2,1)}) %reduce-scatter.5.cloned.1.call-update) | async-done | bytes 393232 | tf_op jit(solution)/shard_map/reduce_scatter | solution.py:189
  400.2 2.1 fusion.5
  (36 shorter events, 4.8 us)
Async XLA Ops:
  7.2 3.3 copy-start.4
  7.2 114.0 %all-gather.3.cloned.1.call-start = ((), (), s32[]{:S(2)}) async-start(), calls=%async_computation.2 | async-start | bytes 3538944 | tf_op jit(solution)/shard_map/all_gather | solution.py:185
  10.4 226.4 %reduce-scatter.3.cloned.1.call-start = ((), (), s32[]{:S(2)}) async-start(), calls=%async_computation.3 | async-start | bytes 3538944 | tf_op jit(solution)/shard_map/reduce_scatter | solution.py:189
  10.8 1.7 copy-start.5
  12.5 2.2 copy-start.8
  16.1 2.9 copy-start.2
  121.2 6.8 %copy-start.3 = (bf16[2048,704]{1,0:T(8,128)(2,1)S(1)}, bf16[2048,704]{1,0:T(8,128)(2,1)}, u32[]{:S(2)}) copy-start(bf16[2048,704]{1,0:T(8,128)(2,1)} %get-tuple-element.42) | copy-start | bytes 8650756
  139.5 1.4 copy-start.6
  139.5 3.6 copy-start.9
  139.6 169.5 %all-gather.5.cloned.1.call-start = ((), (), s32[]{:S(2)}) async-start(), calls=%async_computation.4 | async-start | bytes 3538944 | tf_op jit(solution)/shard_map/all_gather | solution.py:185
  147.2 89.6 %copy-start.1 = (bf16[96,2048]{1,0:T(8,128)(2,1)S(1)}, bf16[96,2048]{1,0:T(8,128)(2,1)}, u32[]{:S(2)}) copy-start(bf16[96,2048]{1,0:T(8,128)(2,1)} %param.9) | copy-start | bytes 1179652
  148.5 91.5 %copy-start.7 = (f32[128,2816]{1,0:T(8,128)S(1)}, f32[128,2816]{1,0:T(8,128)}, u32[]{:S(2)}) copy-start(f32[128,2816]{1,0:T(8,128)} %param.17) | copy-start | bytes 4325380
  240.0 160.2 %reduce-scatter.5.cloned.1.call-start = ((), (), s32[]{:S(2)}) async-start(), calls=%async_computation.5 | async-start | bytes 3538944 | tf_op jit(solution)/shard_map/reduce_scatter | solution.py:189
  287.0 28.7 %copy-start = (bf16[2048,704]{1,0:T(8,128)(2,1)S(1)}, bf16[2048,704]{1,0:T(8,128)(2,1)}, u32[]{:S(2)}) copy-start(bf16[2048,704]{1,0:T(8,128)(2,1)} %relayout.5) | copy-start | bytes 8650756
Sparse Core Ops, SparseCore 0:
  10.7 84.7 all-gather.2
  139.7 97.1 reduce-scatter.2
  240.1 68.8 all-gather.4
  327.4 72.7 reduce-scatter.4
where the time goes:
time: 410 us; the launch traced here: 409 us
  Pallas kernels  216 us (53%)
  waiting for transfers between devices  87.8 us (21%)
  local copies, waits for them, and re-layouts  40.2 us (10%)
  matrix products  36.5 us (9%)
  other arithmetic  14 us (3%)
  between operations  14 us (3%)
    pallas_call x3, Pallas kernels, relayout(): pl.pallas_call(functools.partial(relayout_kernel, sizes), out_shape=[serv...  216 us
    reduce_scatter x2, waiting for transfers between devices, scatter_sum(): return lax.psum_scatter(partial, 'fs', scatter_dimension=0, tiled=True)  65.7 us
    unnamed x29, local copies, waits for them, and re-layouts  29.7 us
    dot_general x2, matrix products, partial_branch(): lax.dot_general(hidden, down_weight, (((1,), (1,)), ((), ())), preferred_...  23.1 us
    all_gather x2, waiting for transfers between devices, gather_tokens(): return lax.all_gather(normed, 'fs', axis=0, tiled=True)  22 us
    dot_general x2, matrix products, partial_branch(): jnp.dot(tokens_in, gate_weight, preferred_element_type=jnp.float32)  13.4 us
  transfers between devices with their start and end apart: 4, of which 3 were waited for; matrix products, arithmetic and copies ran while one was open for 11% of the time, Pallas kernels for 53%

commit v1 on v0

v1 whole, which is shorter than its diff:
```python
import functools

import jax
import jax.numpy as jnp
from jax import lax
from jax.experimental import pallas as pl
from jax.experimental.pallas import tpu as pltpu
from jax.sharding import PartitionSpec as P

EPS = 1e-06
MESH = pl.DeviceIdType.MESH
VMEM_LIMIT = 63 * 1024 * 1024
ANY = pl.BlockSpec(memory_space=pl.ANY)
VMEM = pl.BlockSpec(memory_space=pltpu.VMEM)


def inner_of(fs):
    return max(n for n in range(1, fs + 1) if fs % n == 0 and n * n <= fs)


class Place:
    def __init__(self, sizes):
        self.gr, self.fs, self.tp = sizes
        self.ny = inner_of(self.fs)
        self.nz = self.fs // self.ny
        self.g, self.f, self.t = (lax.axis_index(axis) for axis in ("gr", "fs", "tp"))
        self.z = self.f // self.ny
        self.y = self.f % self.ny

    def at(self, z, y):
        return (self.g, z * self.ny + y, self.t)


def remote(src, dst, send_sem, recv_sem, device):
    return pltpu.make_async_remote_copy(
        src_ref=src,
        dst_ref=dst,
        send_sem=send_sem,
        recv_sem=recv_sem,
        device_id=device,
        device_id_type=MESH,
    )


def wait_bytes(ref, sem):
    pltpu.make_async_copy(ref, ref, sem).wait()


def rows_of_block(ref, f, count):
    return ref.at[pl.ds(pl.multiple_of(f * count, count), count)]


class Relayout:
    def __init__(self, place, pieces, out, sems):
        self.p, self.pieces, self.out = place, pieces, out
        self.first_send, self.first_recv, self.gr_send, self.gr_recv, self.tp_send, self.tp_recv = sems
        self.blocks, self.rows, self.width = pieces.shape
        self.sub = self.rows // place.tp

    def rows_of(self, from_gr, from_fs, core):
        start = pl.multiple_of((from_gr * self.p.fs + from_fs) * self.rows + core * self.sub, self.sub)
        return self.out.at[pl.ds(start, self.sub)]

    def _first(self, step, act_local, act_far):
        p = self.p
        slot = (step + p.f) % self.blocks
        block = p.t * self.blocks + slot
        for core in range(p.tp):
            mine = jnp.logical_and(block == p.f, p.t == core)
            source = self.pieces.at[slot, pl.ds(core * self.sub, self.sub)]
            target = self.rows_of(p.g, p.f, core)
            far = remote(
                source,
                target,
                self.first_send.at[slot, core],
                self.first_recv.at[p.f],
                (p.g, block, core),
            )
            if act_local is not None:

                @pl.when(mine)
                def _():
                    act_local(source, target)

            @pl.when(jnp.logical_not(mine))
            def _():
                act_far(far)

    def send(self):
        def local(source, target):
            pltpu.make_async_copy(source, target, self.first_recv.at[self.p.f]).start()

        def body(step, carry):
            self._first(step, local, lambda copy: copy.start())
            return carry

        lax.fori_loop(0, self.blocks, body, 0)

    def origin(self, step):
        p, blocks = self.p, self.blocks
        return ((p.f // blocks + step % p.tp) % p.tp) * blocks + (p.f + blocks - step // p.tp) % blocks

    def _to_peers(self, ref):
        p = self.p
        for hop in range(1, p.tp):
            remote(ref, ref, self.tp_send, self.tp_recv, (p.g, p.f, (p.t + hop) % p.tp)).start()

    def pass_on(self):
        p = self.p

        def body(step, carry):
            source = self.origin(step)
            ref = self.rows_of(p.g, source, p.t)
            wait_bytes(ref, self.first_recv.at[source])
            for hop in range(1, p.gr):
                remote(
                    ref,
                    ref,
                    self.gr_send,
                    self.gr_recv.at[hop - 1, source],
                    ((p.g + hop) % p.gr, p.f, p.t),
                ).start()
            self._to_peers(ref)
            return carry

        lax.fori_loop(0, p.fs, body, 0)

    def pass_far(self):
        p = self.p

        def body(step, carry):
            source = self.origin(step)
            for hop in range(1, p.gr):
                ref = self.rows_of((p.g + p.gr - hop) % p.gr, source, p.t)
                wait_bytes(ref, self.gr_recv.at[hop - 1, source])
                self._to_peers(ref)
            return carry

        lax.fori_loop(0, p.fs, body, 0)

    def _wait_rows(self, count, sem):
        if count:
            wait_bytes(self.out.at[pl.ds(0, count)], sem)

    def wait_all_here(self):
        p = self.p
        self._wait_rows(p.gr * p.fs * self.sub * (p.tp - 1), self.tp_recv)

    def drain(self):
        p = self.p

        def body(step, carry):
            self._first(step, None, lambda copy: copy.wait_send())
            return carry

        lax.fori_loop(0, self.blocks, body, 0)
        self._wait_rows(p.fs * self.sub * (p.gr - 1), self.gr_send)
        self._wait_rows(p.gr * p.fs * self.sub * (p.tp - 1), self.tp_send)


def relayout_sems(mats, blocks, sizes):
    gr, fs, tp = sizes
    return [
        pltpu.SemaphoreType.DMA((mats, blocks, tp)),
        pltpu.SemaphoreType.DMA((mats, fs)),
        pltpu.SemaphoreType.DMA((mats,)),
        pltpu.SemaphoreType.DMA((mats, max(gr - 1, 1), fs)),
        pltpu.SemaphoreType.DMA((mats,)),
        pltpu.SemaphoreType.DMA((mats,)),
    ]


class Gather:
    def __init__(self, place, tokens, count, send_sem, recv_sem):
        self.p, self.tokens, self.count = place, tokens, count
        self.send_sem, self.recv_sem = send_sem, recv_sem

    def block(self, f):
        return rows_of_block(self.tokens, f, self.count)

    def _copy(self, f, way, z, y):
        ref = self.block(f)
        return remote(ref, ref, self.send_sem.at[f, way], self.recv_sem.at[f], self.p.at(z, y))

    def _forwards(self, z0, y0, dz, dy, act):
        p = self.p
        f = z0 * p.ny + y0
        for sign in dz:
            z = p.z + sign

            @pl.when((z >= 0) & (z < p.nz))
            def _():
                act(self._copy(f, 0 if sign > 0 else 1, z, p.y))

        for sign in dy:
            y = p.y + sign

            @pl.when((y >= 0) & (y < p.ny))
            def _():
                act(self._copy(f, 2 if sign > 0 else 3, p.z, y))

    def _each(self, stage, visit):
        p = self.p
        if stage == 0:
            visit(None, p.z, p.y, (1, -1), (1, -1))
        elif stage < p.nz:
            for sign in (1, -1):
                z0 = p.z - sign * stage
                visit((z0 >= 0) & (z0 < p.nz), z0, p.y, (sign,), (1, -1))
        else:
            hops = stage - p.nz + 1
            for away in range(p.nz):
                for sign_z in (1, -1) if away else (1,):
                    z0 = p.z - sign_z * away
                    for sign in (1, -1):
                        y0 = p.y - sign * hops
                        ways = (sign,) if hops + 1 < p.ny else ()
                        visit((z0 >= 0) & (z0 < p.nz) & (y0 >= 0) & (y0 < p.ny), z0, y0, (), ways)

    def stages(self):
        return self.p.nz + self.p.ny - 1

    def run(self, stage, arrived=None):
        def visit(valid, z0, y0, dz, dy):
            def go():
                f = z0 * self.p.ny + y0
                if stage:
                    wait_bytes(self.block(f), self.recv_sem.at[f])
                self._forwards(z0, y0, dz, dy, lambda copy: copy.start())
                if arrived is not None:
                    arrived(f)

            if valid is None:
                go()
            else:
                pl.when(valid)(go)

        self._each(stage, visit)

    def drain(self):
        def visit(valid, z0, y0, dz, dy):
            def go():
                self._forwards(z0, y0, dz, dy, lambda copy: copy.wait_send())

            if valid is None:
                go()
            else:
                pl.when(valid)(go)

        for stage in range(self.stages()):
            self._each(stage, visit)


class Scatter:
    def __init__(self, place, part, y_land, z_land, count, sems):
        self.p, self.part, self.y_land, self.z_land, self.count = place, part, y_land, z_land, count
        self.y_send, self.y_recv, self.z_send, self.z_recv = sems

    def block(self, f):
        return rows_of_block(self.part, f, self.count)

    def _y_copy(self, z0, y0, sign):
        p = self.p
        f = z0 * p.ny + y0
        at = p.y + sign
        slot = f if sign < 0 else jnp.where(at == y0, p.fs + z0, f)
        return remote(
            self.block(f), self.y_land.at[slot], self.y_send.at[f], self.y_recv.at[slot], p.at(p.z, at)
        )

    def _z_copy(self, z0, sign):
        p = self.p
        at = p.z + sign
        slot = z0 if sign < 0 else jnp.where(at == z0, p.nz, z0)
        return remote(
            self.block(z0 * p.ny + p.y),
            self.z_land.at[slot],
            self.z_send.at[z0],
            self.z_recv.at[slot],
            p.at(at, p.y),
        )

    def _add(self, f, land, recv, slot):
        wait_bytes(land.at[slot], recv.at[slot])
        rows = pl.ds(pl.multiple_of(f * self.count, self.count), self.count)
        total = self.part[rows].astype(jnp.float32) + land[slot].astype(jnp.float32)
        self.part[rows] = total.astype(jnp.bfloat16)

    def send_y(self, z0):
        p = self.p
        for hops in range(p.ny - 1, 0, -1):
            for sign in (1, -1):
                y0, behind = p.y + sign * hops, p.y - sign
                valid = (y0 >= 0) & (y0 < p.ny)
                f = z0 * p.ny + y0
                if hops + 1 < p.ny:

                    @pl.when(valid & (behind >= 0) & (behind < p.ny))
                    def _():
                        self._add(f, self.y_land, self.y_recv, f)

                @pl.when(valid)
                def _():
                    self._y_copy(z0, y0, sign).start()

    def take_y(self, z0):
        p = self.p
        f = z0 * p.ny + p.y

        @pl.when(p.y + 1 < p.ny)
        def _():
            self._add(f, self.y_land, self.y_recv, f)

        @pl.when(p.y > 0)
        def _():
            self._add(f, self.y_land, self.y_recv, p.fs + z0)

    def by_distance(self, visit):
        p = self.p
        for hops in range(p.nz - 1, 0, -1):
            for sign in (1, -1):
                z0 = p.z + sign * hops
                pl.when((z0 >= 0) & (z0 < p.nz))(functools.partial(visit, z0, sign, hops))

    def reduce(self):
        p = self.p

        def step(z0, sign, hops):
            self.take_y(z0)
            behind = p.z - sign
            if hops + 1 < p.nz:

                @pl.when((behind >= 0) & (behind < p.nz))
                def _():
                    self._add(z0 * p.ny + p.y, self.z_land, self.z_recv, z0)

            self._z_copy(z0, sign).start()

        self.by_distance(step)
        self.take_y(p.z)

        @pl.when(p.z + 1 < p.nz)
        def _():
            self._add(p.f, self.z_land, self.z_recv, p.z)

        @pl.when(p.z > 0)
        def _():
            self._add(p.f, self.z_land, self.z_recv, p.nz)

    def drain(self):
        p = self.p
        for z0 in range(p.nz):
            for hops in range(1, p.ny):
                for sign in (1, -1):
                    y0 = p.y + sign * hops

                    @pl.when((y0 >= 0) & (y0 < p.ny))
                    def _():
                        self._y_copy(z0, y0, sign).wait_send()

        self.by_distance(lambda z0, sign, hops: self._z_copy(z0, sign).wait_send())


def scatter_scratch(sizes, count, depth):
    fs = sizes[1]
    ny = inner_of(fs)
    nz = fs // ny
    return [
        pltpu.VMEM((fs + nz, count, depth), jnp.bfloat16),
        pltpu.VMEM((nz + 1, count, depth), jnp.bfloat16),
        pltpu.SemaphoreType.DMA((fs,)),
        pltpu.SemaphoreType.DMA((fs + nz,)),
        pltpu.SemaphoreType.DMA((nz,)),
        pltpu.SemaphoreType.DMA((nz + 1,)),
    ]


def normed_tokens(resid_f):
    return (
        resid_f * lax.rsqrt(jnp.mean(resid_f * resid_f, axis=-1, keepdims=True) + EPS)
    ).astype(jnp.bfloat16)


def column_of(row):
    n = row.shape[1]
    across = lax.broadcasted_iota(jnp.int32, (n, n), 1)
    down = lax.broadcasted_iota(jnp.int32, (n, n), 0)
    return jnp.sum(jnp.where(across == down, row, 0.0), axis=1, keepdims=True)


def cut_into(pieces, weight, gain):
    blocks, _, width = pieces.shape
    for slot in range(blocks):
        value = weight[:, slot * width : (slot + 1) * width]
        if gain is not None:
            value = gain * value
        pieces[slot] = value.astype(jnp.bfloat16)


def ffn_rows(tokens, weights, part, hidden, start, scales):
    gate, up, down = weights
    in_scale, out_scale = scales
    count, width = hidden.shape
    depth = tokens.shape[1]
    rows = pl.ds(start, count)
    for low in range(0, width, 256):
        high = min(low + 256, width)
        gate_pre = jnp.dot(tokens[rows, :], gate[:, low:high], preferred_element_type=jnp.float32) * in_scale
        up_pre = jnp.dot(tokens[rows, :], up[:, low:high], preferred_element_type=jnp.float32) * in_scale
        act = gate_pre / (1.0 + jnp.exp(-gate_pre)) * up_pre
        hidden[:, low:high] = act.astype(jnp.bfloat16)
    chunk = 256 if depth % 256 == 0 else depth

    def body(i, carry):
        low = pl.multiple_of(i * chunk, chunk)
        value = lax.dot_general(
            hidden[...],
            down[pl.ds(low, chunk), :],
            (((1,), (1,)), ((), ())),
            preferred_element_type=jnp.float32,
        )
        part[rows, pl.ds(low, chunk)] = (value * out_scale).astype(jnp.bfloat16)
        return carry

    lax.fori_loop(0, depth // chunk, body, 0)


def scales_of(depth, width, fs):
    return depth ** (-0.5), (width * fs) ** (-0.5)


def first_kernel(sizes, count, rows_at_once, *refs):
    (prompt, gain_first, gain_second, *weights), refs = refs[:9], refs[9:]
    (*served, tokens_out, middle_out), refs = refs[:8], refs[8:]
    (prompt_v, weights_v, pieces, first_v, tokens, tokens_next, part, hidden), refs = refs[:8], refs[8:]
    (in_sem, out_sem, token_sem, ag_send, ag_recv, *refs) = refs
    relayout_refs, scatter_refs = refs[:6], refs[6:]
    p = Place(sizes)
    total, width = served[0].shape
    depth = tokens.shape[1]
    scales = scales_of(depth, width, p.fs)

    loads = [pltpu.make_async_copy(prompt, prompt_v, in_sem.at[6])]
    loads += [pltpu.make_async_copy(weights[m], weights_v.at[m], in_sem.at[m]) for m in range(6)]
    for load in loads:
        load.start()

    targets = [first_v.at[m] for m in range(3)] + list(served[3:])
    moves = [
        Relayout(p, pieces.at[m], targets[m], [s.at[m] for s in relayout_refs]) for m in range(6)
    ]
    gains = [gain_first, gain_first, None, gain_second, gain_second, None]

    def cut(m):
        loads[1 + m].wait()
        gain = None if gains[m] is None else column_of(gains[m][...])
        cut_into(pieces.at[m], weights_v.at[m], gain)

    own = pl.ds(pl.multiple_of(p.f * count, count), count)
    gather = Gather(p, tokens, count, ag_send.at[0], ag_recv.at[0])
    loads[0].wait()
    tokens[own] = normed_tokens(prompt_v[...].astype(jnp.float32))
    gather.run(0)
    cut(0)
    moves[0].send()
    cut(1)
    gather.run(1)
    moves[1].send()
    cut(2)
    moves[0].pass_on()
    for stage in range(2, p.nz - 1):
        gather.run(stage)
    moves[2].send()
    moves[1].pass_on()
    for stage in range(max(p.nz - 1, 2), p.nz):
        gather.run(stage)
    cut(3)
    cut(4)
    cut(5)
    moves[2].pass_on()
    for stage in range(p.nz, gather.stages()):
        gather.run(stage)
    for m in range(3):
        moves[m].pass_far()
    for m in range(3):
        moves[m].wait_all_here()
    outs = [pltpu.make_async_copy(first_v.at[m], served[m], out_sem.at[m]) for m in range(3)]
    for out in outs:
        out.start()
    moves[3].send()

    scatter = Scatter(p, part, scatter_refs[0], scatter_refs[1], count, scatter_refs[2:])
    blocks_at_once = rows_at_once // count
    tiles = p.fs // blocks_at_once
    z_at_once = blocks_at_once // p.ny

    def tile(step, carry):
        at = (tiles - 1 - step) if tiles == 1 else jnp.where(2 * p.z < p.nz, tiles - 1 - step, step)
        start = pl.multiple_of(at * rows_at_once, rows_at_once)
        ffn_rows(tokens, [first_v.at[m] for m in range(3)], part, hidden, start, scales)
        for i in range(z_at_once):
            scatter.send_y(at * z_at_once + jnp.where(2 * p.z < p.nz, z_at_once - 1 - i, i))
        return carry

    lax.fori_loop(0, tiles, tile, 0)
    moves[4].send()
    scatter.reduce()
    middle = (prompt_v[...].astype(jnp.float32) + 0.5 * part[own].astype(jnp.float32)).astype(jnp.bfloat16)
    middle_out[...] = middle
    tokens_next[own] = normed_tokens(middle.astype(jnp.float32))
    gather_next = Gather(p, tokens_next, count, ag_send.at[1], ag_recv.at[1])

    def store(f):
        pltpu.make_async_copy(
            rows_of_block(tokens_next, f, count), rows_of_block(tokens_out, f, count), token_sem
        ).start()

    gather_next.run(0, store)
    moves[3].pass_on()
    for stage in range(1, p.nz):
        if stage == 1:
            moves[5].send()
        gather_next.run(stage, store)
        if stage == 2:
            moves[4].pass_on()
    moves[5].pass_on()
    for stage in range(p.nz, gather_next.stages()):
        gather_next.run(stage, store)
    for m in range(3, 6):
        moves[m].pass_far()
    for m in range(3, 6):
        moves[m].wait_all_here()
    wait_bytes(tokens_next, token_sem)
    for out in outs:
        out.wait()
    for move in moves:
        move.drain()
    gather.drain()
    gather_next.drain()
    scatter.drain()


def first_half(prompt, gains, weights, sizes):
    gr, fs, tp = sizes
    rows, columns = weights[0].shape
    count, depth = prompt.shape
    blocks = fs // tp
    width = columns // blocks
    total = gr * fs * rows
    rows_at_once = count * fs // 2
    bf16 = jnp.bfloat16
    served = jax.ShapeDtypeStruct((total, width), bf16)
    return pl.pallas_call(
        functools.partial(first_kernel, sizes, count, rows_at_once),
        out_shape=[served] * 6
        + [jax.ShapeDtypeStruct((count * fs, depth), bf16), jax.ShapeDtypeStruct((count, depth), bf16)],
        in_specs=[ANY, VMEM, VMEM] + [ANY] * 6,
        out_specs=[ANY] * 7 + [VMEM],
        scratch_shapes=[
            pltpu.VMEM((count, depth), bf16),
            pltpu.VMEM((6, rows, columns), jnp.float32),
            pltpu.VMEM((6, blocks, rows, width), bf16),
            pltpu.VMEM((3, total, width), bf16),
            pltpu.VMEM((count * fs, depth), bf16),
            pltpu.VMEM((count * fs, depth), bf16),
            pltpu.VMEM((count * fs, depth), bf16),
            pltpu.VMEM((rows_at_once, width), bf16),
            pltpu.SemaphoreType.DMA((7,)),
            pltpu.SemaphoreType.DMA((3,)),
            pltpu.SemaphoreType.DMA,
            pltpu.SemaphoreType.DMA((2, fs, 4)),
            pltpu.SemaphoreType.DMA((2, fs)),
            *relayout_sems(6, blocks, sizes),
            *scatter_scratch(sizes, count, depth),
        ],
        compiler_params=pltpu.CompilerParams(has_side_effects=True, vmem_limit_bytes=VMEM_LIMIT),
        name="first_half",
    )(prompt, *(gain.reshape(1, -1) for gain in gains), *weights)


def second_kernel(fs, rows_at_once, *refs):
    (tokens, *served), refs = refs[:7], refs[7:]
    (*outs, part), refs = refs[:7], refs[7:]
    tokens_v, served_v, part_v, hidden, in_sem, out_sem, part_sem = refs
    order = [3, 4, 5, 0, 1, 2]
    depth, width = tokens.shape[1], served[0].shape[1]
    scales = scales_of(depth, width, fs)
    loads = {m: pltpu.make_async_copy(served[m], served_v.at[m], in_sem.at[m]) for m in order}
    stores = {m: pltpu.make_async_copy(served_v.at[m], outs[m], out_sem.at[m]) for m in order}
    load_tokens = pltpu.make_async_copy(tokens, tokens_v, in_sem.at[6])
    load_tokens.start()
    for m in order:
        loads[m].start()
    load_tokens.wait()
    for m in order[:3]:
        loads[m].wait()
        stores[m].start()
    tiles = tokens.shape[0] // rows_at_once

    def tile(step, carry):
        start = pl.multiple_of(step * rows_at_once, rows_at_once)
        ffn_rows(tokens_v, [served_v.at[m] for m in (3, 4, 5)], part_v, hidden, start, scales)
        rows = pl.ds(start, rows_at_once)
        pltpu.make_async_copy(part_v.at[rows], part.at[rows], part_sem).start()
        return carry

    lax.fori_loop(0, tiles, tile, 0)
    for m in order[3:]:
        loads[m].wait()
        stores[m].start()
    for m in order:
        stores[m].wait()
    wait_bytes(part_v, part_sem)


def second_half(tokens, served, fs):
    total, width = served[0].shape
    count, depth = tokens.shape
    rows_at_once = count // 2
    bf16 = jnp.bfloat16
    return pl.pallas_call(
        functools.partial(second_kernel, fs, rows_at_once),
        out_shape=[jax.ShapeDtypeStruct((total, width), bf16)] * 6
        + [jax.ShapeDtypeStruct((count, depth), bf16)],
        in_specs=[ANY] * 7,
        out_specs=[ANY] * 7,
        scratch_shapes=[
            pltpu.VMEM((count, depth), bf16),
            pltpu.VMEM((6, total, width), bf16),
            pltpu.VMEM((count, depth), bf16),
            pltpu.VMEM((rows_at_once, width), bf16),
            pltpu.SemaphoreType.DMA((7,)),
            pltpu.SemaphoreType.DMA((6,)),
            pltpu.SemaphoreType.DMA,
        ],
        compiler_params=pltpu.CompilerParams(vmem_limit_bytes=VMEM_LIMIT),
        name="second_half",
    )(tokens, *served)


def last_kernel(sizes, count, partial, middle, result, part, part_sem, *scatter_refs):
    p = Place(sizes)
    scatter = Scatter(p, part, scatter_refs[0], scatter_refs[1], count, scatter_refs[2:])

    def load(z0):
        rows = pl.ds(pl.multiple_of(z0 * p.ny * count, p.ny * count), p.ny * count)
        return pltpu.make_async_copy(partial.at[rows], part.at[rows], part_sem.at[z0])

    order = []
    for i in range(p.nz):
        order.append(jnp.where(2 * p.z < p.nz, p.nz - 1 - i, i))
    for z0 in order:
        load(z0).start()
    for z0 in order:
        load(z0).wait()
        scatter.send_y(z0)
    scatter.reduce()
    own = pl.ds(pl.multiple_of(p.f * count, count), count)
    result[...] = (
        middle[...].astype(jnp.float32) + 0.5 * part[own].astype(jnp.float32)
    ).astype(jnp.bfloat16)
    scatter.drain()


def last_step(partial, middle, sizes):
    fs = sizes[1]
    count, depth = middle.shape
    return pl.pallas_call(
        functools.partial(last_kernel, sizes, count),
        out_shape=jax.ShapeDtypeStruct((count, depth), jnp.bfloat16),
        in_specs=[ANY, VMEM],
        out_specs=VMEM,
        scratch_shapes=[
            pltpu.VMEM((fs * count, depth), jnp.bfloat16),
            pltpu.SemaphoreType.DMA((fs // inner_of(fs),)),
            *scatter_scratch(sizes, count, depth),
        ],
        compiler_params=pltpu.CompilerParams(has_side_effects=True, vmem_limit_bytes=VMEM_LIMIT),
        name="last_step",
    )(partial, middle)


def on_device(
    prompt,
    norm_first,
    gate_first,
    up_first,
    down_first,
    norm_second,
    gate_second,
    up_second,
    down_second,
):
    sizes = tuple(lax.axis_size(axis) for axis in ("gr", "fs", "tp"))
    weights = (gate_first, up_first, down_first, gate_second, up_second, down_second)
    *served, tokens, middle = first_half(prompt, (norm_first, norm_second), weights, sizes)
    *served, partial = second_half(tokens, served, sizes[1])
    result = last_step(partial, middle, sizes)
    return (*served, result)


def solution(mesh):
    in_specs = (
        P(("gr", "fs", "tp"), None),
        P(("gr", "fs")),
        P(("gr", "fs"), "tp"),
        P(("gr", "fs"), "tp"),
        P(("gr", "fs"), "tp"),
        P(("gr", "fs")),
        P(("gr", "fs"), "tp"),
        P(("gr", "fs"), "tp"),
        P(("gr", "fs"), "tp"),
    )
    out_specs = (
        P(None, "fs"),
        P(None, "fs"),
        P(None, "fs"),
        P(None, "fs"),
        P(None, "fs"),
        P(None, "fs"),
        P(("gr", "fs", "tp"), None),
    )
    return jax.shard_map(
        on_device, mesh=mesh, in_specs=in_specs, out_specs=out_specs, check_vma=False
    )
```

time: 410 us -> 328 us (0.80)
  Pallas kernels: 216 us -> 304 us
  waiting for transfers between devices: 87.8 us -> 0 us
  matrix products: 36.5 us -> 0 us
  local copies, waits for them, and re-layouts: 40.2 us -> 23 us
  other arithmetic: 14 us -> 0 us
  between operations: 14 us -> 0.67 us
    pallas_call x3, Pallas kernels: 216 us -> 304 us  [the longest x1 224 us: first_half(): pl.pallas_call(functools.partial(first_kernel, sizes, count, rows_at_once...]
    reduce_scatter x2 -> x0, waiting for transfers between devices: 65.7 us -> none  [scatter_sum(): return lax.psum_scatter(partial, 'fs', scatter_dimension=0, tiled=True)]
    dot_general x4 -> x0, matrix products: 36.5 us -> none  [the longest x2 23.1 us: partial_branch(): lax.dot_general(hidden, down_weight, (((1,), (1,)), ((), ())), preferred_...]
    all_gather x2 -> x0, waiting for transfers between devices: 22 us -> none  [gather_tokens(): return lax.all_gather(normed, 'fs', axis=0, tiled=True)]
    convert_element_type x5 -> x0, other arithmetic: 8.48 us -> none  [the longest x2 3.78 us: normed_tokens(): return (resid_f * lax.rsqrt(jnp.mean(resid_f * resid_f, axis=-1, keepdims...]
    reshape x6 -> x0, local copies, waits for them, and re-layouts: 7.94 us -> none  [cut(): m.reshape(rows, blocks, columns // blocks).transpose(1, 0, 2)]
    unnamed x29 -> x15, local copies, waits for them, and re-layouts: 29.7 us -> 23 us
  transfers between devices with their start and end apart: 4 -> 0, of which waited for: 3 -> 0; matrix products, arithmetic and copies ran while one was open for 11% -> 0% of each run, Pallas kernels for 53% -> 0%
where the time goes in v1:
time: 328 us
  Pallas kernels  304 us (93%)
  local copies, waits for them, and re-layouts  23 us (7%)
    pallas_call x1, Pallas kernels, first_half(): pl.pallas_call(functools.partial(first_kernel, sizes, count, rows_at_once...  224 us
    pallas_call x1, Pallas kernels, last_step(): pl.pallas_call(functools.partial(last_kernel, sizes, count), out_shape=ja...  58.4 us
    unnamed x15, local copies, waits for them, and re-layouts  23 us
    pallas_call x1, Pallas kernels, second_half(): pl.pallas_call(functools.partial(second_kernel, fs, rows_at_once), out_sh...  22 us

profile of v1, /device:TPU:0, one launch (start us, length us, event | category | flops | bytes accessed | tf_op | source)
XLA Modules:
  0.0 327.8 jit_solution(4928861113649514457)
XLA Ops:
  0.6 223.8 %first_half.1 = (bf16[2048,704]{1,0:T(8,128)(2,1)}, bf16[2048,704]{1,0:T(8,128)(2,1)}, bf16[2048,704]{1,0:T(8,128)(2,1)}, bf16[2048,704]{1,0:T(8,128)(2,1)}, bf1...) custom-call(bf16[96,2048]{1,0:T(8,128)(2,1)} %refs_0_.1, ...), custom_call_target="tpu_custom_call" | custom-call | tf_op jit(solution)/shard_map/first_half/pallas_call | solution.py:553
  224.4 22.0 %second_half.1 = (bf16[2048,704]{1,0:T(8,128)(2,1)}, bf16[2048,704]{1,0:T(8,128)(2,1)}, bf16[2048,704]{1,0:T(8,128)(2,1)}, bf16[2048,704]{1,0:T(8,128)(2,1)}, bf...) custom-call(bf16[768,2048]{1,0:T(8,128)(2,1)} %get-tuple-element.22.refs_0_, ...), custom_call_target="tpu_custom_call" | custom-call | tf_op jit(solution)/shard_map/second_half/pallas_call | solution.py:621
  246.4 58.4 %last_step.1 = bf16[96,2048]{1,0:T(8,128)(2,1)} custom-call(bf16[768,2048]{1,0:T(8,128)(2,1)} %get-tuple-element.35.partial, bf16[96,2048]{1,0:T(8,128)(2,1)} %get-tuple-element.36.middle), custom_call_target="tpu_custom_call" | custom-call | tf_op jit(solution)/shard_map/last_step/pallas_call | solution.py:668
  304.9 0.0 copy-start.2
  304.9 4.7 %copy.16 = bf16[2048,704]{0,1:T(8,128)(2,1)} copy(bf16[2048,704]{1,0:T(8,128)(2,1)} %get-tuple-element.37) | data formatting | bytes 5767168
  309.6 0.0 copy-done.2
  309.6 2.7 copy.17
  312.3 0.0 copy-start.1
  312.3 4.7 %copy.18 = bf16[2048,704]{0,1:T(8,128)(2,1)} copy(bf16[2048,704]{1,0:T(8,128)(2,1)} %get-tuple-element.39) | data formatting | bytes 5767168
  317.0 0.0 copy-done.1
  317.0 2.7 copy.19
  319.7 0.0 copy-start
  319.7 4.7 %copy.20 = bf16[2048,704]{0,1:T(8,128)(2,1)} copy(bf16[2048,704]{1,0:T(8,128)(2,1)} %get-tuple-element.41) | data formatting | bytes 5767168
  324.4 0.0 copy-done
  324.4 0.0 copy-start.3
  324.4 2.7 copy.21
  327.1 0.0 copy-done.3
  327.1 0.7 copy.23
Async XLA Ops:
  304.9 4.7 %copy-start.2 = (bf16[2048,704]{1,0:T(8,128)(2,1)S(1)}, bf16[2048,704]{1,0:T(8,128)(2,1)}, u32[]{:S(2)}) copy-start(bf16[2048,704]{1,0:T(8,128)(2,1)} %get-tuple-element.38) | copy-start | bytes 8650756
  312.3 4.7 %copy-start.1 = (bf16[2048,704]{1,0:T(8,128)(2,1)S(1)}, bf16[2048,704]{1,0:T(8,128)(2,1)}, u32[]{:S(2)}) copy-start(bf16[2048,704]{1,0:T(8,128)(2,1)} %get-tuple-element.40) | copy-start | bytes 8650756
  319.7 4.7 %copy-start = (bf16[2048,704]{1,0:T(8,128)(2,1)S(1)}, bf16[2048,704]{1,0:T(8,128)(2,1)}, u32[]{:S(2)}) copy-start(bf16[2048,704]{1,0:T(8,128)(2,1)} %get-tuple-element.42) | copy-start | bytes 8650756
  324.4 2.7 copy-start.3

commit v2 on v1

v2 whole, which is shorter than its diff:
```python
import functools

import jax
import jax.numpy as jnp
from jax import lax
from jax.experimental import pallas as pl
from jax.experimental.pallas import tpu as pltpu
from jax.sharding import PartitionSpec as P

EPS = 1e-06
MESH = pl.DeviceIdType.MESH
VMEM_LIMIT = 63 * 1024 * 1024
CUTS = 2
SAME, NEAR, ACROSS = range(3)
ANY = pl.BlockSpec(memory_space=pl.ANY)
VMEM = pl.BlockSpec(memory_space=pltpu.VMEM)


def inner_of(fs):
    return max(n for n in range(1, fs + 1) if fs % n == 0 and n * n <= fs)


class Place:
    def __init__(self, sizes):
        self.gr, self.fs, self.tp = sizes
        self.ny = inner_of(self.fs)
        self.nz = self.fs // self.ny
        self.g, self.f, self.t = (lax.axis_index(axis) for axis in ("gr", "fs", "tp"))
        self.z = self.f // self.ny
        self.y = self.f % self.ny

    def at(self, z, y):
        return (self.g, z * self.ny + y, self.t)

    def partner(self, z):
        return z + 1 - 2 * (z % 2)

    def by_z(self, z, z0, cut):
        paired = z0 == self.partner(z)
        return paired if cut == 0 else paired & (z > 0) & (z < self.nz - 1)


def remote(src, dst, send_sem, recv_sem, device):
    return pltpu.make_async_remote_copy(
        src_ref=src,
        dst_ref=dst,
        send_sem=send_sem,
        recv_sem=recv_sem,
        device_id=device,
        device_id_type=MESH,
    )


def wait_bytes(ref, sem):
    pltpu.make_async_copy(ref, ref, sem).wait()


def rows_of_block(ref, f, count):
    return ref.at[pl.ds(pl.multiple_of(f * count, count), count)]


def greet(devices):
    barrier = pltpu.get_barrier_semaphore()
    expected = 0
    for valid, device in devices:

        def signal():
            pl.semaphore_signal(barrier, inc=1, device_id=device, device_id_type=MESH)

        if valid is True:
            signal()
            expected = expected + 1
        else:
            pl.when(valid)(signal)
            expected = expected + jnp.where(valid, 1, 0)
    return lambda: pl.semaphore_wait(barrier, expected)


def plane_and_replicas(p):
    for away in range(p.fs):
        for hop in range(p.tp):
            if away or hop:
                yield True, (p.g, (p.f + away) % p.fs, (p.t + hop) % p.tp)
    for hop in range(1, p.gr):
        yield True, ((p.g + hop) % p.gr, p.f, p.t)


def neighbours(p):
    for sign in (1, -1):
        yield (p.z + sign >= 0) & (p.z + sign < p.nz), p.at(p.z + sign, p.y)
        yield (p.y + sign >= 0) & (p.y + sign < p.ny), p.at(p.z, p.y + sign)


class Relayout:
    def __init__(self, place, turned, pieces, out, sems):
        self.p, self.turned, self.pieces, self.out = place, turned, pieces, out
        self.first_send, self.first_recv, self.gr_send, self.gr_recv, self.tp_send, self.tp_recv = sems
        self.blocks, height, across = pieces.shape
        self.sub = height // place.tp
        self.rows = across if turned else height

    def rows_of(self, from_gr, from_fs, core):
        source = from_gr * self.p.fs + from_fs
        if self.turned:
            start = pl.multiple_of(source * self.rows, self.rows)
            return self.out.at[pl.ds(core * self.sub, self.sub), pl.ds(start, self.rows)]
        start = pl.multiple_of(source * self.rows + core * self.sub, self.sub)
        return self.out.at[pl.ds(start, self.sub)]

    def _first(self, step, act_local, act_far, group):
        p = self.p
        slot = (step + p.f) % self.blocks
        block = p.t * self.blocks + slot
        z0 = block // p.ny
        across = (2 * z0 < p.nz) != (2 * p.z < p.nz)
        if group == SAME:
            wanted = z0 == p.z
        elif group == ACROSS:
            wanted = across
        elif group == NEAR:
            wanted = jnp.logical_not(across) & (z0 != p.z)
        for core in range(p.tp):
            mine = jnp.logical_and(block == p.f, p.t == core)
            source = self.pieces.at[slot, pl.ds(core * self.sub, self.sub)]
            target = self.rows_of(p.g, p.f, core)
            far = remote(
                source,
                target,
                self.first_send.at[slot, core],
                self.first_recv.at[p.f],
                (p.g, block, core),
            )
            if act_local is not None and group == SAME:

                @pl.when(mine)
                def _():
                    act_local(source, target)

            others = jnp.logical_not(mine)

            @pl.when(others if group is None else others & wanted)
            def _():
                act_far(far)

    @jax.named_scope("w_send")
    def send(self, group):
        def local(source, target):
            pltpu.make_async_copy(source, target, self.first_recv.at[self.p.f]).start()

        def body(step, carry):
            self._first(step, local, lambda copy: copy.start(), group)
            return carry

        lax.fori_loop(0, self.blocks, body, 0)

    def _to_peers(self, ref):
        p = self.p
        for hop in range(1, p.tp):
            remote(ref, ref, self.tp_send, self.tp_recv, (p.g, p.f, (p.t + hop) % p.tp)).start()

    def _near(self, hops, visit):
        p = self.p
        for sign in (1, -1) if hops else (1,):
            z0 = p.z + sign * hops

            @pl.when((z0 >= 0) & (z0 < p.nz))
            def _():
                def body(i, carry):
                    visit(z0 * p.ny + (p.y + i) % p.ny)
                    return carry

                lax.fori_loop(0, p.ny, body, 0)

    def pass_on(self, hops):
        p = self.p

        def visit(source):
            ref = self.rows_of(p.g, source, p.t)
            wait_bytes(ref, self.first_recv.at[source])
            for hop in range(1, p.gr):
                remote(
                    ref,
                    ref,
                    self.gr_send,
                    self.gr_recv.at[hop - 1, source],
                    ((p.g + hop) % p.gr, p.f, p.t),
                ).start()
            self._to_peers(ref)

        with jax.named_scope(f"w_pass_on#d={hops}"):
            self._near(hops, visit)

    def pass_far(self, hops):
        p = self.p

        def visit(source):
            for hop in range(1, p.gr):
                ref = self.rows_of((p.g + p.gr - hop) % p.gr, source, p.t)
                wait_bytes(ref, self.gr_recv.at[hop - 1, source])
                self._to_peers(ref)

        with jax.named_scope(f"w_pass_far#d={hops}"):
            self._near(hops, visit)

    def _wait_pieces(self, count, sem):
        if not count:
            return
        if self.turned:
            half = pl.ds(0, self.sub)
            per_row = self.p.gr * self.p.fs
            if count % per_row:
                wait_bytes(self.out.at[half, pl.ds(0, count * self.rows)], sem)
            else:
                wait_bytes(self.out.at[pl.ds(0, self.sub * (count // per_row))], sem)
        else:
            wait_bytes(self.out.at[pl.ds(0, count * self.sub)], sem)

    @jax.named_scope("w_wait")
    def wait_all_here(self):
        p = self.p
        self._wait_pieces(p.gr * p.fs * (p.tp - 1), self.tp_recv)

    def drain(self):
        p = self.p

        def body(step, carry):
            self._first(step, None, lambda copy: copy.wait_send(), None)
            return carry

        lax.fori_loop(0, self.blocks, body, 0)
        self._wait_pieces(p.fs * (p.gr - 1), self.gr_send)
        self._wait_pieces(p.gr * p.fs * (p.tp - 1), self.tp_send)


def relayout_sems(mats, blocks, sizes):
    gr, fs, tp = sizes
    return [
        pltpu.SemaphoreType.DMA((mats, blocks, tp)),
        pltpu.SemaphoreType.DMA((mats, fs)),
        pltpu.SemaphoreType.DMA((mats,)),
        pltpu.SemaphoreType.DMA((mats, max(gr - 1, 1), fs)),
        pltpu.SemaphoreType.DMA((mats,)),
        pltpu.SemaphoreType.DMA((mats,)),
    ]


class Gather:
    def __init__(self, place, tokens, cuts, send_sem, recv_sem):
        self.p, self.tokens, self.cuts = place, tokens, cuts
        self.height = tokens.shape[0] // (place.fs * cuts)
        self.send_sem, self.recv_sem = send_sem, recv_sem

    def piece(self, f, cut):
        return rows_of_block(self.tokens, f * self.cuts + cut, self.height)

    def _along_z(self, f, cut, sign, act, also=None):
        p = self.p
        z = p.z + sign
        ref = self.piece(f, cut)
        valid = (z >= 0) & (z < p.nz)

        @pl.when(valid if also is None else valid & also)
        def _():
            way = jnp.where(sign > 0, 0, 1)
            act(remote(ref, ref, self.send_sem.at[f, cut, way], self.recv_sem.at[f, cut], p.at(z, p.y)))

    def _along_y(self, f, cut, sign, act, also=None):
        p = self.p
        y = p.y + sign
        ref = self.piece(f, cut)
        valid = (y >= 0) & (y < p.ny)

        @pl.when(valid if also is None else valid & also)
        def _():
            way = 2 if sign > 0 else 3
            act(remote(ref, ref, self.send_sem.at[f, cut, way], self.recv_sem.at[f, cut], p.at(p.z, y)))

    def _each(self, stage, arrive, act, done):
        p = self.p
        last = p.nz

        def column(z0, sign, cut):
            f = z0 * p.ny + p.y
            arrive(f, cut)
            self._along_z(f, cut, sign, act)
            by_y = jnp.logical_not(p.by_z(p.z, z0, cut))
            for way in (1, -1):
                self._along_y(f, cut, way, act, by_y)
            done(f, cut)

        def row(z0, y0, sign, hops, same, cut):
            f = z0 * p.ny + y0
            arrive(f, cut)
            if hops + 1 < p.ny:
                self._along_y(f, cut, sign, act, jnp.logical_not(p.by_z(p.z, z0, cut)))
            if same:
                other = p.partner(p.z)
                self._along_z(f, cut, other - p.z, act, p.by_z(other, p.z, cut))
            done(f, cut)

        def rows(away):
            for hops in range(1, p.ny):
                for sign_z in (1, -1) if away else (1,):
                    z0 = p.z - sign_z * away
                    for sign in (1, -1):
                        y0 = p.y - sign * hops

                        @pl.when((z0 >= 0) & (z0 < p.nz) & (y0 >= 0) & (y0 < p.ny))
                        def _():
                            for cut in range(self.cuts):
                                row(z0, y0, sign, hops, away == 0, cut)

        if stage == 0:
            for cut in range(self.cuts):
                for sign in (1, -1):
                    self._along_z(p.f, cut, sign, act)
                    self._along_y(p.f, cut, sign, act)
                done(p.f, cut)
        elif stage < last:
            for sign in (1, -1):
                z0 = p.z - sign * stage

                @pl.when((z0 >= 0) & (z0 < p.nz))
                def _():
                    for cut in range(self.cuts):
                        column(z0, sign, cut)

            if stage == 1:
                rows(0)
        else:
            for away in range(1, p.nz):
                rows(away)

    def run(self, stage, done=lambda f, cut: None):
        with jax.named_scope(f"gather#s={stage}"):
            self._each(
                stage,
                lambda f, cut: wait_bytes(self.piece(f, cut), self.recv_sem.at[f, cut]),
                lambda copy: copy.start(),
                done,
            )

    def drain(self):
        for stage in range(self.p.nz + 1):
            self._each(stage, lambda f, cut: None, lambda copy: copy.wait_send(), lambda f, cut: None)


class Scatter:
    def __init__(self, place, part, y_land, z_land, row_land, sems):
        self.p, self.part, self.y_land, self.z_land, self.row_land = place, part, y_land, z_land, row_land
        self.y_send, self.y_recv, self.z_send, self.z_recv, self.row_recv = sems
        self.cuts, self.height = y_land.shape[1:3]
        self.towards = jnp.where(2 * place.z < place.nz, 1, -1)

    def rows(self, f, cut):
        return pl.ds(pl.multiple_of((f * self.cuts + cut) * self.height, self.height), self.height)

    def _y_copy(self, z0, y0, sign, cut):
        p = self.p
        f = z0 * p.ny + y0
        at = p.y + sign
        slot = f if sign < 0 else jnp.where(at == y0, p.fs + z0, f)
        return remote(
            self.part.at[self.rows(f, cut)],
            self.y_land.at[slot, cut],
            self.y_send.at[f, cut],
            self.y_recv.at[slot, cut],
            p.at(p.z, at),
        )

    def _z_copy(self, z0, sign, cut):
        p = self.p
        at = p.z + sign
        slot = jnp.where((sign > 0) & (at == z0), p.nz, z0)
        return remote(
            self.part.at[self.rows(z0 * p.ny + p.y, cut)],
            self.z_land.at[slot, cut],
            self.z_send.at[z0, cut],
            self.z_recv.at[slot, cut],
            p.at(at, p.y),
        )

    def _add(self, f, land, recv, slot, cut):
        wait_bytes(land.at[slot, cut], recv.at[slot, cut])
        rows = self.rows(f, cut)
        total = self.part[rows].astype(jnp.float32) + land[slot, cut].astype(jnp.float32)
        self.part[rows] = total.astype(jnp.bfloat16)

    def _row_copy(self, z0, y0, cut):
        p = self.p
        f = z0 * p.ny + y0
        return remote(
            self.part.at[self.rows(f, cut)],
            self.row_land.at[y0, cut],
            self.y_send.at[f, cut],
            self.row_recv.at[y0, cut],
            p.at(z0, p.y),
        )

    def send_y(self, z0):
        self._send_y(z0, False)

    def send_own_y(self):
        with jax.named_scope("own_row"):
            self._send_y(self.p.z, True)

    def _send_y(self, z0, own):
        p = self.p
        other = p.partner(p.z)
        for hops in range(p.ny - 1, 0, -1):
            for sign in (1, -1):
                y0, behind = p.y + sign * hops, p.y - sign
                valid = (y0 >= 0) & (y0 < p.ny)
                f = z0 * p.ny + y0
                for cut in range(self.cuts):
                    if own:

                        @pl.when(valid & (other < p.nz) & p.by_z(other, p.z, cut))
                        def _():
                            self._add(f, self.row_land, self.row_recv, y0, cut)

                    by_z = False if own else p.by_z(p.z, z0, cut)
                    by_y = valid if own else valid & jnp.logical_not(by_z)
                    if hops + 1 < p.ny:

                        @pl.when(by_y & (behind >= 0) & (behind < p.ny))
                        def _():
                            self._add(f, self.y_land, self.y_recv, f, cut)

                    @pl.when(by_y)
                    def _():
                        self._y_copy(z0, y0, sign, cut).start()

                    if not own:

                        @pl.when(valid & by_z)
                        def _():
                            self._row_copy(z0, y0, cut).start()

    def take_y(self, z0, cut):
        p = self.p
        f = z0 * p.ny + p.y
        by_y = jnp.logical_not(p.by_z(p.z, z0, cut))

        @pl.when(by_y & (p.y + 1 < p.ny))
        def _():
            self._add(f, self.y_land, self.y_recv, f, cut)

        @pl.when(by_y & (p.y > 0))
        def _():
            self._add(f, self.y_land, self.y_recv, p.fs + z0, cut)

    def at_distance(self, hops, visit, also=None):
        p = self.p
        for sign in (self.towards, -self.towards) if hops else (1,):
            z0 = p.z + sign * hops
            valid = (z0 >= 0) & (z0 < p.nz)
            if also is not None:
                valid = valid & also(z0)
            pl.when(valid)(functools.partial(visit, z0, sign))

    def send_y_of(self, also):
        for hops in range(self.p.nz - 1, 0, -1):
            self.at_distance(hops, lambda z0, sign: self.send_y(z0), also)

    def reduce(self, hops):
        p = self.p

        def step(z0, sign):
            behind = p.z - sign
            for cut in range(self.cuts):
                self.take_y(z0, cut)
                if hops + 1 < p.nz:

                    @pl.when((behind >= 0) & (behind < p.nz))
                    def _():
                        self._add(z0 * p.ny + p.y, self.z_land, self.z_recv, z0, cut)

                self._z_copy(z0, sign, cut).start()

        with jax.named_scope(f"reduce#d={hops}"):
            if hops:
                self.at_distance(hops, step)
                return
            for cut in range(self.cuts):
                self.take_y(p.z, cut)

                @pl.when(p.z + 1 < p.nz)
                def _():
                    self._add(p.f, self.z_land, self.z_recv, p.z, cut)

                @pl.when(p.z > 0)
                def _():
                    self._add(p.f, self.z_land, self.z_recv, p.nz, cut)

    def drain(self):
        p = self.p
        for cut in range(self.cuts):
            for z0 in range(p.nz):
                for hops in range(1, p.ny):
                    for sign in (1, -1):
                        y0 = p.y + sign * hops

                        @pl.when((y0 >= 0) & (y0 < p.ny))
                        def _():
                            self._y_copy(z0, y0, sign, cut).wait_send()

            for hops in range(1, p.nz):
                self.at_distance(hops, lambda z0, sign: self._z_copy(z0, sign, cut).wait_send())


def cuts_of(count):
    return CUTS if count % (16 * CUTS) == 0 else 1


def scatter_scratch(sizes, count, depth):
    fs = sizes[1]
    ny = inner_of(fs)
    nz = fs // ny
    cuts = cuts_of(count)
    piece = (cuts, count // cuts, depth)
    return [
        pltpu.VMEM((fs + nz, *piece), jnp.bfloat16),
        pltpu.VMEM((nz + 1, *piece), jnp.bfloat16),
        pltpu.VMEM((ny, *piece), jnp.bfloat16),
        pltpu.SemaphoreType.DMA((fs, cuts)),
        pltpu.SemaphoreType.DMA((fs + nz, cuts)),
        pltpu.SemaphoreType.DMA((nz, cuts)),
        pltpu.SemaphoreType.DMA((nz + 1, cuts)),
        pltpu.SemaphoreType.DMA((ny, cuts)),
    ]


def normed_tokens(resid_f):
    return (
        resid_f * lax.rsqrt(jnp.mean(resid_f * resid_f, axis=-1, keepdims=True) + EPS)
    ).astype(jnp.bfloat16)


def column_of(row):
    n = row.shape[1]
    across = lax.broadcasted_iota(jnp.int32, (n, n), 1)
    down = lax.broadcasted_iota(jnp.int32, (n, n), 0)
    return jnp.sum(jnp.where(across == down, row, 0.0), axis=1, keepdims=True)


@jax.named_scope("cut")
def cut_into(pieces, weight, gain, turned):
    blocks, height, width = pieces.shape
    if turned:
        value = weight[...].T
        if gain is not None:
            value = value * gain[...]
        for slot in range(blocks):
            pieces[slot] = value[slot * height : (slot + 1) * height].astype(jnp.bfloat16)
        return
    gain = None if gain is None else column_of(gain[...])
    for slot in range(blocks):
        value = weight[:, slot * width : (slot + 1) * width]
        if gain is not None:
            value = gain * value
        pieces[slot] = value.astype(jnp.bfloat16)


def slabs_of(width):
    return [(low, min(low + 256, width)) for low in range(0, width, 256)]


@jax.named_scope("ffn")
def ffn_rows(tokens, weights, part, hidden, start, scales, turned, ready=lambda i: None):
    gate, up, down = weights
    in_scale, out_scale = scales
    count, width = hidden.shape
    depth = tokens.shape[1]
    rows = pl.ds(start, count)
    inward = (((1,), (1 if turned else 0,)), ((), ()))
    outward = (((1,), (0 if turned else 1,)), ((), ()))
    for i, (low, high) in enumerate(slabs_of(width)):
        ready(i)

        def project(weight):
            block = weight[low:high, :] if turned else weight[:, low:high]
            return lax.dot_general(
                tokens[rows, :], block, inward, preferred_element_type=jnp.float32
            ) * in_scale

        gate_pre, up_pre = project(gate), project(up)
        act = gate_pre / (1.0 + jnp.exp(-gate_pre)) * up_pre
        hidden[:, low:high] = act.astype(jnp.bfloat16)
    ready(None)
    chunk = 256 if depth % 256 == 0 else depth

    def body(i, carry):
        low = pl.multiple_of(i * chunk, chunk)
        block = down[:, pl.ds(low, chunk)] if turned else down[pl.ds(low, chunk), :]
        value = lax.dot_general(hidden[...], block, outward, preferred_element_type=jnp.float32)
        part[rows, pl.ds(low, chunk)] = (value * out_scale).astype(jnp.bfloat16)
        return carry

    lax.fori_loop(0, depth // chunk, body, 0)


def scales_of(depth, width, fs):
    return depth ** (-0.5), (width * fs) ** (-0.5)


def turns(rows):
    return rows % 128 == 0


def first_kernel(sizes, count, rows_at_once, turned, *refs):
    (prompt, gain_first, gain_second, *weights), refs = refs[:9], refs[9:]
    (*served, tokens_out, middle_out), refs = refs[:8], refs[8:]
    (prompt_v, weights_v, pieces, first_v, tokens, tokens_next, part, hidden), refs = refs[:8], refs[8:]
    (in_sem, out_sem, token_sem, ag_send, ag_recv, *refs) = refs
    relayout_refs, scatter_refs = refs[:6], refs[6:]
    p = Place(sizes)
    depth = tokens.shape[1]
    scales = scales_of(depth, hidden.shape[1], p.fs)

    loads = [pltpu.make_async_copy(prompt, prompt_v, in_sem.at[6])]
    loads += [pltpu.make_async_copy(weights[m], weights_v.at[m], in_sem.at[m]) for m in range(6)]
    with jax.named_scope("start"):
        for load in loads:
            load.start()

    targets = [first_v.at[m] for m in range(3)] + list(served[3:])
    moves = [
        Relayout(p, turned, pieces.at[m], targets[m], [s.at[m] for s in relayout_refs])
        for m in range(6)
    ]
    gains = [gain_first, gain_first, None, gain_second, gain_second, None]

    def cut(m):
        loads[1 + m].wait()
        cut_into(pieces.at[m], weights_v.at[m], gains[m], turned)

    own = pl.ds(pl.multiple_of(p.f * count, count), count)
    cuts = cuts_of(count)
    gather = Gather(p, tokens, cuts, ag_send.at[0], ag_recv.at[0])
    stages = range(p.nz)
    arrive = greet(plane_and_replicas(p))
    loads[0].wait()
    tokens[own] = normed_tokens(prompt_v[...].astype(jnp.float32))
    cut(0)
    with jax.named_scope("barrier"):
        arrive()

    def send(m):
        for group in (ACROSS, SAME, NEAR):
            moves[m].send(group)

    send(0)
    gather.run(0)
    for m in range(1, 3):
        cut(m)
    send(1)
    for hops in stages:
        moves[0].pass_on(hops)
    gather.run(1)
    send(2)
    for hops in stages[:2]:
        moves[1].pass_on(hops)
    for stage in stages[2:3]:
        gather.run(stage)
    for hops in stages[2:]:
        moves[1].pass_on(hops)
    for hops in stages[:2]:
        moves[2].pass_on(hops)
    for stage in stages[3:]:
        gather.run(stage)
    for m in range(3, 6):
        cut(m)
    for hops in stages[2:]:
        moves[2].pass_on(hops)
    gather.run(p.nz)
    for m in range(3, 6):
        send(m)
    for m in range(3):
        for hops in stages:
            moves[m].pass_far(hops)
    for m in range(3):
        moves[m].wait_all_here()
    outs = [pltpu.make_async_copy(first_v.at[m], served[m], out_sem.at[m]) for m in range(3)]
    for out in outs:
        out.start()

    scatter = Scatter(p, part, *scatter_refs[:3], scatter_refs[3:])
    blocks_at_once = rows_at_once // count
    tiles = p.fs // blocks_at_once
    z_at_once = blocks_at_once // p.ny

    def tile(step, carry):
        at = jnp.where(2 * p.z < p.nz, tiles - 1 - step, step)
        start = pl.multiple_of(at * rows_at_once, rows_at_once)
        ffn_rows(tokens, [first_v.at[m] for m in range(3)], part, hidden, start, scales, turned)
        scatter.send_y_of(lambda z0: z0 // z_at_once == at)
        return carry

    lax.fori_loop(0, tiles, tile, 0)
    for hops in stages:
        moves[3].pass_on(hops)
    for hops in reversed(stages):
        scatter.reduce(hops)
        if hops == min(2, p.nz - 1):
            scatter.send_own_y()
        for m in range(4, 6):
            if hops == p.nz + 3 - m:
                for d in stages:
                    moves[m].pass_on(d)
    middle = (prompt_v[...].astype(jnp.float32) + 0.5 * part[own].astype(jnp.float32)).astype(jnp.bfloat16)
    middle_out[...] = middle
    tokens_next[own] = normed_tokens(middle.astype(jnp.float32))
    gather_next = Gather(p, tokens_next, cuts, ag_send.at[1], ag_recv.at[1])

    def store(f, cut):
        piece, height = f * cuts + cut, count // cuts
        pltpu.make_async_copy(
            rows_of_block(tokens_next, piece, height), rows_of_block(tokens_out, piece, height), token_sem
        ).start()

    for stage in range(p.nz + 1):
        gather_next.run(stage, store)
    for m in range(3, 6):
        for hops in stages:
            moves[m].pass_far(hops)
    for m in range(3, 6):
        moves[m].wait_all_here()
    wait_bytes(tokens_next, token_sem)
    for out in outs:
        out.wait()
    for move in moves:
        move.drain()
    gather.drain()
    gather_next.drain()
    scatter.drain()


def first_half(prompt, gains, weights, sizes):
    gr, fs, tp = sizes
    rows, columns = weights[0].shape
    count, depth = prompt.shape
    blocks = fs // tp
    width = columns // blocks
    total = gr * fs * rows
    rows_at_once = count * fs // 2
    bf16 = jnp.bfloat16
    turned = turns(rows)
    across = (width, total) if turned else (total, width)
    piece = (width, rows) if turned else (rows, width)
    served = jax.ShapeDtypeStruct(across, bf16)
    return pl.pallas_call(
        functools.partial(first_kernel, sizes, count, rows_at_once, turned),
        out_shape=[served] * 6
        + [jax.ShapeDtypeStruct((count * fs, depth), bf16), jax.ShapeDtypeStruct((count, depth), bf16)],
        in_specs=[ANY, VMEM, VMEM] + [ANY] * 6,
        out_specs=[ANY] * 7 + [VMEM],
        scratch_shapes=[
            pltpu.VMEM((count, depth), bf16),
            pltpu.VMEM((6, rows, columns), jnp.float32),
            pltpu.VMEM((6, blocks, *piece), bf16),
            pltpu.VMEM((3, *across), bf16),
            pltpu.VMEM((count * fs, depth), bf16),
            pltpu.VMEM((count * fs, depth), bf16),
            pltpu.VMEM((count * fs, depth), bf16),
            pltpu.VMEM((rows_at_once, width), bf16),
            pltpu.SemaphoreType.DMA((7,)),
            pltpu.SemaphoreType.DMA((3,)),
            pltpu.SemaphoreType.DMA,
            pltpu.SemaphoreType.DMA((2, fs, cuts_of(count), 4)),
            pltpu.SemaphoreType.DMA((2, fs, cuts_of(count))),
            *relayout_sems(6, blocks, sizes),
            *scatter_scratch(sizes, count, depth),
        ],
        compiler_params=pltpu.CompilerParams(
            collective_id=0, has_side_effects=True, vmem_limit_bytes=VMEM_LIMIT
        ),
        name="first_half",
    )(prompt, *(gain.reshape(1, -1) for gain in gains), *weights)


def second_kernel(fs, rows_at_once, turned, *refs):
    (tokens, *served), refs = refs[:7], refs[7:]
    (*outs, part), refs = refs[:7], refs[7:]
    tokens_v, served_v, part_v, hidden, in_sem, out_sem, part_sem = refs
    width = hidden.shape[1]
    scales = scales_of(tokens.shape[1], width, fs)
    loads = {m: pltpu.make_async_copy(served[m], served_v.at[m], in_sem.at[m]) for m in (0, 1, 2, 5)}
    stores = [pltpu.make_async_copy(served_v.at[m], outs[m], out_sem.at[m]) for m in range(6)]

    def load_slab(m, i, low, high):
        slab = (pl.ds(low, high - low),) if turned else (slice(None), pl.ds(low, high - low))
        return pltpu.make_async_copy(served[m].at[slab], served_v.at[(m, *slab)], in_sem.at[7 + 2 * i + m - 3])

    slabs = slabs_of(width) if turned else [(0, width)]
    load_tokens = pltpu.make_async_copy(tokens, tokens_v, in_sem.at[6])
    load_tokens.start()
    for i, (low, high) in enumerate(slabs):
        for m in (3, 4):
            load_slab(m, i, low, high).start()
    for m in (5, 0, 1, 2):
        loads[m].start()
    load_tokens.wait()
    tiles = tokens.shape[0] // rows_at_once

    def tile(step, carry):
        def ready(i):
            @pl.when(step == 0)
            def _():
                if i is None:
                    loads[5].wait()
                elif i < len(slabs):
                    for m in (3, 4):
                        load_slab(m, i, *slabs[i]).wait()

        start = pl.multiple_of(step * rows_at_once, rows_at_once)
        weights = [served_v.at[m] for m in (3, 4, 5)]
        ffn_rows(tokens_v, weights, part_v, hidden, start, scales, turned, ready)
        rows = pl.ds(start, rows_at_once)
        pltpu.make_async_copy(part_v.at[rows], part.at[rows], part_sem).start()

        @pl.when(step == 0)
        def _():
            for m in range(3):
                loads[m].wait()
            for store in stores:
                store.start()

        return carry

    lax.fori_loop(0, tiles, tile, 0)
    wait_bytes(part_v, part_sem)
    for store in stores:
        store.wait()


def second_half(tokens, served, fs, turned):
    across = served[0].shape
    width = across[0 if turned else 1]
    count, depth = tokens.shape
    rows_at_once = count // 2
    bf16 = jnp.bfloat16
    return pl.pallas_call(
        functools.partial(second_kernel, fs, rows_at_once, turned),
        out_shape=[jax.ShapeDtypeStruct(across, bf16)] * 6
        + [jax.ShapeDtypeStruct((count, depth), bf16)],
        in_specs=[ANY] * 7,
        out_specs=[ANY] * 7,
        scratch_shapes=[
            pltpu.VMEM((count, depth), bf16),
            pltpu.VMEM((6, *across), bf16),
            pltpu.VMEM((count, depth), bf16),
            pltpu.VMEM((rows_at_once, width), bf16),
            pltpu.SemaphoreType.DMA((7 + 2 * len(slabs_of(width)),)),
            pltpu.SemaphoreType.DMA((6,)),
            pltpu.SemaphoreType.DMA,
        ],
        compiler_params=pltpu.CompilerParams(vmem_limit_bytes=VMEM_LIMIT),
        name="second_half",
    )(tokens, *served)


def last_kernel(sizes, count, partial, middle, result, part, part_sem, *scatter_refs):
    p = Place(sizes)
    scatter = Scatter(p, part, *scatter_refs[:3], scatter_refs[3:])

    def load(z0):
        rows = pl.ds(pl.multiple_of(z0 * p.ny * count, p.ny * count), p.ny * count)
        return pltpu.make_async_copy(partial.at[rows], part.at[rows], part_sem.at[z0])

    def begin(z0, sign):
        load(z0).wait()
        scatter.send_y(z0)

    arrive = greet(neighbours(p))
    for hops in range(p.nz - 1, -1, -1):
        scatter.at_distance(hops, lambda z0, sign: load(z0).start())
    arrive()
    for hops in range(p.nz - 1, 0, -1):
        scatter.at_distance(hops, begin)
    load(p.z).wait()
    for hops in range(p.nz - 1, -1, -1):
        scatter.reduce(hops)
        if hops == min(2, p.nz - 1):
            scatter.send_own_y()
    own = pl.ds(pl.multiple_of(p.f * count, count), count)
    result[...] = (
        middle[...].astype(jnp.float32) + 0.5 * part[own].astype(jnp.float32)
    ).astype(jnp.bfloat16)
    scatter.drain()


def last_step(partial, middle, sizes):
    fs = sizes[1]
    count, depth = middle.shape
    return pl.pallas_call(
        functools.partial(last_kernel, sizes, count),
        out_shape=jax.ShapeDtypeStruct((count, depth), jnp.bfloat16),
        in_specs=[ANY, VMEM],
        out_specs=VMEM,
        scratch_shapes=[
            pltpu.VMEM((fs * count, depth), jnp.bfloat16),
            pltpu.SemaphoreType.DMA((fs // inner_of(fs),)),
            *scatter_scratch(sizes, count, depth),
        ],
        compiler_params=pltpu.CompilerParams(
            collective_id=1, has_side_effects=True, vmem_limit_bytes=VMEM_LIMIT
        ),
        name="last_step",
    )(partial, middle)


def on_device(
    prompt,
    norm_first,
    gate_first,
    up_first,
    down_first,
    norm_second,
    gate_second,
    up_second,
    down_second,
):
    sizes = tuple(lax.axis_size(axis) for axis in ("gr", "fs", "tp"))
    weights = (gate_first, up_first, down_first, gate_second, up_second, down_second)
    *served, tokens, middle = first_half(prompt, (norm_first, norm_second), weights, sizes)
    turned = turns(gate_first.shape[0])
    *served, partial = second_half(tokens, served, sizes[1], turned)
    result = last_step(partial, middle, sizes)
    if turned:
        served = [block.T for block in served]
    return (*served, result)


def solution(mesh):
    in_specs = (
        P(("gr", "fs", "tp"), None),
        P(("gr", "fs")),
        P(("gr", "fs"), "tp"),
        P(("gr", "fs"), "tp"),
        P(("gr", "fs"), "tp"),
        P(("gr", "fs")),
        P(("gr", "fs"), "tp"),
        P(("gr", "fs"), "tp"),
        P(("gr", "fs"), "tp"),
    )
    out_specs = (
        P(None, "fs"),
        P(None, "fs"),
        P(None, "fs"),
        P(None, "fs"),
        P(None, "fs"),
        P(None, "fs"),
        P(("gr", "fs", "tp"), None),
    )
    return jax.shard_map(
        on_device, mesh=mesh, in_specs=in_specs, out_specs=out_specs, check_vma=False
    )
```

time: 328 us -> 246 us (0.75)
  Pallas kernels: 304 us -> 243 us
  local copies, waits for them, and re-layouts: 23 us -> 1.77 us
    pallas_call x1, Pallas kernels: 224 us -> 189 us  [first_half(): pl.pallas_call(functools.partial(first_kernel, sizes, count, rows_at_once...]
    unnamed x15 -> x1, local copies, waits for them, and re-layouts: 23 us -> 1.77 us
    pallas_call x1, Pallas kernels: 58.4 us -> 39 us  [last_step(): pl.pallas_call(functools.partial(last_kernel, sizes, count), out_shape=ja...]
    pallas_call x1, Pallas kernels: 22 us -> 15.5 us  [second_half(): pl.pallas_call(functools.partial(second_kernel, fs, rows_at_once, turned)...]
where the time goes in v2:
time: 246 us; the launch traced here: 245 us
  Pallas kernels  243 us (99%)
    pallas_call x1, Pallas kernels, first_half(): pl.pallas_call(functools.partial(first_kernel, sizes, count, rows_at_once...  189 us
    pallas_call x1, Pallas kernels, last_step(): pl.pallas_call(functools.partial(last_kernel, sizes, count), out_shape=ja...  39 us
    pallas_call x1, Pallas kernels, second_half(): pl.pallas_call(functools.partial(second_kernel, fs, rows_at_once, turned)...  15.5 us

profile of v2, /device:TPU:0, one launch (start us, length us, event | category | flops | bytes accessed | tf_op | source)
XLA Modules:
  0.0 245.4 jit_solution(1999749364340672677)
XLA Ops:
  0.6 188.5 %first_half.1 = (bf16[704,2048]{1,0:T(8,128)(2,1)}, bf16[704,2048]{1,0:T(8,128)(2,1)}, bf16[704,2048]{1,0:T(8,128)(2,1)}, bf16[704,2048]{1,0:T(8,128)(2,1)}, bf1...) custom-call(bf16[96,2048]{1,0:T(8,128)(2,1)} %refs_0_.1, ...), custom_call_target="tpu_custom_call" | custom-call | tf_op jit(solution)/shard_map/first_half/pallas_call | solution.py:752
  189.2 15.5 %second_half.1 = (bf16[704,2048]{1,0:T(8,128)(2,1)}, bf16[704,2048]{1,0:T(8,128)(2,1)}, bf16[704,2048]{1,0:T(8,128)(2,1)}, bf16[704,2048]{1,0:T(8,128)(2,1)}, bf...) custom-call(bf16[768,2048]{1,0:T(8,128)(2,1)} %get-tuple-element.22.refs_0_, ...), custom_call_target="tpu_custom_call" | custom-call | tf_op jit(solution)/shard_map/second_half/pallas_call | solution.py:843
  204.6 39.0 %last_step.1 = bf16[96,2048]{1,0:T(8,128)(2,1)} custom-call(bf16[768,2048]{1,0:T(8,128)(2,1)} %get-tuple-element.35.partial, bf16[96,2048]{1,0:T(8,128)(2,1)} %get-tuple-element.36.middle), custom_call_target="tpu_custom_call" | custom-call | tf_op jit(solution)/shard_map/last_step/pallas_call | solution.py:896
  243.6 1.8 copy.17

commit v3 on v2

--- a/solution.py
+++ b/solution.py
@@ -10,7 +10,7 @@
 EPS = 1e-06
 MESH = pl.DeviceIdType.MESH
 VMEM_LIMIT = 63 * 1024 * 1024
-CUTS = 2
+CUTS = 3
 SAME, NEAR, ACROSS = range(3)
 ANY = pl.BlockSpec(memory_space=pl.ANY)
 VMEM = pl.BlockSpec(memory_space=pltpu.VMEM)
@@ -32,12 +32,15 @@
     def at(self, z, y):
         return (self.g, z * self.ny + y, self.t)
 
+    def same_half(self, z0):
+        return (2 * z0 < self.nz) == (2 * self.z < self.nz)
+
     def partner(self, z):
         return z + 1 - 2 * (z % 2)
 
-    def by_z(self, z, z0, cut):
+    def by_z(self, z, z0, cut, ends=True):
         paired = z0 == self.partner(z)
-        return paired if cut == 0 else paired & (z > 0) & (z < self.nz - 1)
+        return paired if ends and cut == 0 else paired & (z > 0) & (z < self.nz - 1)
 
 
 def remote(src, dst, send_sem, recv_sem, device):
@@ -85,12 +88,6 @@
         yield True, ((p.g + hop) % p.gr, p.f, p.t)
 
 
-def neighbours(p):
-    for sign in (1, -1):
-        yield (p.z + sign >= 0) & (p.z + sign < p.nz), p.at(p.z + sign, p.y)
-        yield (p.y + sign >= 0) & (p.y + sign < p.ny), p.at(p.z, p.y + sign)
-
-
 class Relayout:
     def __init__(self, place, turned, pieces, out, sems):
         self.p, self.turned, self.pieces, self.out = place, turned, pieces, out
@@ -112,7 +109,7 @@
         slot = (step + p.f) % self.blocks
         block = p.t * self.blocks + slot
         z0 = block // p.ny
-        across = (2 * z0 < p.nz) != (2 * p.z < p.nz)
+        across = jnp.logical_not(p.same_half(z0))
         if group == SAME:
             wanted = z0 == p.z
         elif group == ACROSS:
@@ -158,20 +155,21 @@
         for hop in range(1, p.tp):
             remote(ref, ref, self.tp_send, self.tp_recv, (p.g, p.f, (p.t + hop) % p.tp)).start()
 
-    def _near(self, hops, visit):
-        p = self.p
-        for sign in (1, -1) if hops else (1,):
-            z0 = p.z + sign * hops
-
-            @pl.when((z0 >= 0) & (z0 < p.nz))
-            def _():
-                def body(i, carry):
-                    visit(z0 * p.ny + (p.y + i) % p.ny)
-                    return carry
-
-                lax.fori_loop(0, p.ny, body, 0)
-
-    def pass_on(self, hops):
+    def _sources(self, groups, visit):
+        p = self.p
+
+        def body(i, carry):
+            source = (p.f + 2 * p.fs - i // p.tp - (i % p.tp) * self.blocks) % p.fs
+            z0 = source // p.ny
+            same, half = z0 == p.z, p.same_half(z0)
+            kinds = {SAME: same, NEAR: half & jnp.logical_not(same), ACROSS: jnp.logical_not(half)}
+            wanted = functools.reduce(jnp.logical_or, [kinds[group] for group in groups])
+            pl.when(wanted)(functools.partial(visit, source))
+            return carry
+
+        lax.fori_loop(0, p.fs, body, 0)
+
+    def pass_on(self, *groups):
         p = self.p
 
         def visit(source):
@@ -187,10 +185,10 @@
                 ).start()
             self._to_peers(ref)
 
-        with jax.named_scope(f"w_pass_on#d={hops}"):
-            self._near(hops, visit)
-
-    def pass_far(self, hops):
+        with jax.named_scope(f"w_pass_on#{groups}"):
+            self._sources(groups, visit)
+
+    def pass_far(self, *groups):
         p = self.p
 
         def visit(source):
@@ -199,8 +197,8 @@
                 wait_bytes(ref, self.gr_recv.at[hop - 1, source])
                 self._to_peers(ref)
 
-        with jax.named_scope(f"w_pass_far#d={hops}"):
-            self._near(hops, visit)
+        with jax.named_scope(f"w_pass_far#{groups}"):
+            self._sources(groups, visit)
 
     def _wait_pieces(self, count, sem):
         if not count:
@@ -245,8 +243,8 @@
 
 
 class Gather:
-    def __init__(self, place, tokens, cuts, send_sem, recv_sem):
-        self.p, self.tokens, self.cuts = place, tokens, cuts
+    def __init__(self, place, tokens, cuts, ends, send_sem, recv_sem):
+        self.p, self.tokens, self.cuts, self.ends = place, tokens, cuts, ends
         self.height = tokens.shape[0] // (place.fs * cuts)
         self.send_sem, self.recv_sem = send_sem, recv_sem
 
@@ -275,7 +273,7 @@
             way = 2 if sign > 0 else 3
             act(remote(ref, ref, self.send_sem.at[f, cut, way], self.recv_sem.at[f, cut], p.at(p.z, y)))
 
-    def _each(self, stage, arrive, act, done):
+    def _each(self, stage, half, arrive, act, done):
         p = self.p
         last = p.nz
 
@@ -283,7 +281,7 @@
             f = z0 * p.ny + p.y
             arrive(f, cut)
             self._along_z(f, cut, sign, act)
-            by_y = jnp.logical_not(p.by_z(p.z, z0, cut))
+            by_y = jnp.logical_not(p.by_z(p.z, z0, cut, self.ends))
             for way in (1, -1):
                 self._along_y(f, cut, way, act, by_y)
             done(f, cut)
@@ -292,10 +290,10 @@
             f = z0 * p.ny + y0
             arrive(f, cut)
             if hops + 1 < p.ny:
-                self._along_y(f, cut, sign, act, jnp.logical_not(p.by_z(p.z, z0, cut)))
+                self._along_y(f, cut, sign, act, jnp.logical_not(p.by_z(p.z, z0, cut, self.ends)))
             if same:
                 other = p.partner(p.z)
-                self._along_z(f, cut, other - p.z, act, p.by_z(other, p.z, cut))
+                self._along_z(f, cut, other - p.z, act, p.by_z(other, p.z, cut, self.ends))
             done(f, cut)
 
         def rows(away):
@@ -320,21 +318,26 @@
             for sign in (1, -1):
                 z0 = p.z - sign * stage
 
-                @pl.when((z0 >= 0) & (z0 < p.nz))
+                valid = (z0 >= 0) & (z0 < p.nz)
+                if half is not None:
+                    valid = valid & (p.same_half(z0) if half else jnp.logical_not(p.same_half(z0)))
+
+                @pl.when(valid)
                 def _():
                     for cut in range(self.cuts):
                         column(z0, sign, cut)
 
-            if stage == 1:
+            if stage == 1 and half is not False:
                 rows(0)
         else:
             for away in range(1, p.nz):
                 rows(away)
 
-    def run(self, stage, done=lambda f, cut: None):
+    def run(self, stage, done=lambda f, cut: None, half=None):
         with jax.named_scope(f"gather#s={stage}"):
             self._each(
                 stage,
+                half,
                 lambda f, cut: wait_bytes(self.piece(f, cut), self.recv_sem.at[f, cut]),
                 lambda copy: copy.start(),
                 done,
@@ -342,7 +345,7 @@
 
     def drain(self):
         for stage in range(self.p.nz + 1):
-            self._each(stage, lambda f, cut: None, lambda copy: copy.wait_send(), lambda f, cut: None)
+            self._each(stage, None, lambda f, cut: None, lambda copy: copy.wait_send(), lambda f, cut: None)
 
 
 class Scatter:
@@ -608,11 +611,11 @@
     return rows % 128 == 0
 
 
-def first_kernel(sizes, count, rows_at_once, turned, *refs):
+def main_kernel(sizes, count, rows_at_once, turned, *refs):
     (prompt, gain_first, gain_second, *weights), refs = refs[:9], refs[9:]
-    (*served, tokens_out, middle_out), refs = refs[:8], refs[8:]
-    (prompt_v, weights_v, pieces, first_v, tokens, tokens_next, part, hidden), refs = refs[:8], refs[8:]
-    (in_sem, out_sem, token_sem, ag_send, ag_recv, *refs) = refs
+    (*served, result), refs = refs[:7], refs[7:]
+    (prompt_v, weights_v, pieces, served_v, tokens, tokens_next, part, hidden, middle_v), refs = refs[:9], refs[9:]
+    (in_sem, out_sem, ag_send, ag_recv, *refs) = refs
     relayout_refs, scatter_refs = refs[:6], refs[6:]
     p = Place(sizes)
     depth = tokens.shape[1]
@@ -624,9 +627,8 @@
         for load in loads:
             load.start()
 
-    targets = [first_v.at[m] for m in range(3)] + list(served[3:])
     moves = [
-        Relayout(p, turned, pieces.at[m], targets[m], [s.at[m] for s in relayout_refs])
+        Relayout(p, turned, pieces.at[m], served_v.at[m], [s.at[m] for s in relayout_refs])
         for m in range(6)
     ]
     gains = [gain_first, gain_first, None, gain_second, gain_second, None]
@@ -637,7 +639,7 @@
 
     own = pl.ds(pl.multiple_of(p.f * count, count), count)
     cuts = cuts_of(count)
-    gather = Gather(p, tokens, cuts, ag_send.at[0], ag_recv.at[0])
+    gather = Gather(p, tokens, cuts, False, ag_send.at[0], ag_recv.at[0])
     stages = range(p.nz)
     arrive = greet(plane_and_replicas(p))
     loads[0].wait()
@@ -646,97 +648,111 @@
     with jax.named_scope("barrier"):
         arrive()
 
-    def send(m):
-        for group in (ACROSS, SAME, NEAR):
+    def send(m, *groups):
+        for group in groups or (ACROSS, SAME, NEAR):
             moves[m].send(group)
 
     send(0)
     gather.run(0)
     for m in range(1, 3):
         cut(m)
-    send(1)
-    for hops in stages:
-        moves[0].pass_on(hops)
-    gather.run(1)
-    send(2)
-    for hops in stages[:2]:
-        moves[1].pass_on(hops)
+    send(1, SAME, NEAR)
+    send(2, SAME)
+    moves[0].pass_on(SAME)
+    gather.run(1, half=True)
+    send(1, ACROSS)
+    moves[0].pass_on(NEAR)
+    moves[0].pass_on(ACROSS)
+    moves[1].pass_on(SAME, NEAR)
+    gather.run(1, half=False)
+    send(2, ACROSS, NEAR)
+    moves[2].pass_on(SAME)
+    for m in range(3, 6):
+        cut(m)
     for stage in stages[2:3]:
         gather.run(stage)
-    for hops in stages[2:]:
-        moves[1].pass_on(hops)
-    for hops in stages[:2]:
-        moves[2].pass_on(hops)
+    moves[2].pass_on(NEAR)
+    moves[1].pass_on(ACROSS)
     for stage in stages[3:]:
         gather.run(stage)
-    for m in range(3, 6):
-        cut(m)
-    for hops in stages[2:]:
-        moves[2].pass_on(hops)
-    gather.run(p.nz)
+    moves[0].pass_far(SAME, NEAR, ACROSS)
+    moves[2].pass_on(ACROSS)
     for m in range(3, 6):
         send(m)
-    for m in range(3):
-        for hops in stages:
-            moves[m].pass_far(hops)
+    gather.run(p.nz)
+    for m in range(1, 3):
+        moves[m].pass_far(SAME, NEAR)
+        moves[m].pass_far(ACROSS)
     for m in range(3):
         moves[m].wait_all_here()
-    outs = [pltpu.make_async_copy(first_v.at[m], served[m], out_sem.at[m]) for m in range(3)]
-    for out in outs:
-        out.start()
+    outs = [pltpu.make_async_copy(served_v.at[m], served[m], out_sem.at[m]) for m in range(6)]
+    for m in range(3):
+        outs[m].start()
 
     scatter = Scatter(p, part, *scatter_refs[:3], scatter_refs[3:])
-    blocks_at_once = rows_at_once // count
-    tiles = p.fs // blocks_at_once
-    z_at_once = blocks_at_once // p.ny
-
-    def tile(step, carry):
-        at = jnp.where(2 * p.z < p.nz, tiles - 1 - step, step)
-        start = pl.multiple_of(at * rows_at_once, rows_at_once)
-        ffn_rows(tokens, [first_v.at[m] for m in range(3)], part, hidden, start, scales, turned)
-        scatter.send_y_of(lambda z0: z0 // z_at_once == at)
-        return carry
-
-    lax.fori_loop(0, tiles, tile, 0)
-    for hops in stages:
-        moves[3].pass_on(hops)
+    tiles = p.fs * count // rows_at_once
+    z_at_once = p.nz // tiles
+
+    def branch(source, first_weight):
+        def tile(step, carry):
+            at = jnp.where(2 * p.z < p.nz, tiles - 1 - step, step)
+            start = pl.multiple_of(at * rows_at_once, rows_at_once)
+            weights = [served_v.at[first_weight + m] for m in range(3)]
+            ffn_rows(source, weights, part, hidden, start, scales, turned)
+            scatter.send_y_of(lambda z0: z0 // z_at_once == at)
+            return carry
+
+        lax.fori_loop(0, tiles, tile, 0)
+
+    branch(tokens, 0)
+    moves[3].pass_on(SAME, NEAR)
+    moves[3].pass_on(ACROSS)
     for hops in reversed(stages):
         scatter.reduce(hops)
         if hops == min(2, p.nz - 1):
             scatter.send_own_y()
-        for m in range(4, 6):
-            if hops == p.nz + 3 - m:
-                for d in stages:
-                    moves[m].pass_on(d)
+        if hops == p.nz - 1:
+            moves[4].pass_on(SAME, NEAR)
+            moves[4].pass_on(ACROSS)
+        if hops == min(2, p.nz - 1):
+            moves[5].pass_on(SAME, NEAR)
+            moves[5].pass_on(ACROSS)
     middle = (prompt_v[...].astype(jnp.float32) + 0.5 * part[own].astype(jnp.float32)).astype(jnp.bfloat16)
-    middle_out[...] = middle
+    middle_v[...] = middle
     tokens_next[own] = normed_tokens(middle.astype(jnp.float32))
-    gather_next = Gather(p, tokens_next, cuts, ag_send.at[1], ag_recv.at[1])
-
-    def store(f, cut):
-        piece, height = f * cuts + cut, count // cuts
-        pltpu.make_async_copy(
-            rows_of_block(tokens_next, piece, height), rows_of_block(tokens_out, piece, height), token_sem
-        ).start()
-
-    for stage in range(p.nz + 1):
-        gather_next.run(stage, store)
-    for m in range(3, 6):
-        for hops in stages:
-            moves[m].pass_far(hops)
+    gather_next = Gather(p, tokens_next, cuts, True, ag_send.at[1], ag_recv.at[1])
+    gather_next.run(0)
+    for m in range(3, 5):
+        moves[m].pass_far(SAME, NEAR, ACROSS)
+    for stage in stages[1:]:
+        gather_next.run(stage)
+        if stage == 1:
+            moves[5].pass_far(SAME, NEAR, ACROSS)
+    gather_next.run(p.nz)
     for m in range(3, 6):
         moves[m].wait_all_here()
-    wait_bytes(tokens_next, token_sem)
-    for out in outs:
-        out.wait()
-    for move in moves:
-        move.drain()
-    gather.drain()
-    gather_next.drain()
+    for m in range(3, 6):
+        outs[m].start()
     scatter.drain()
-
-
-def first_half(prompt, gains, weights, sizes):
+    branch(tokens_next, 3)
+    for hops in reversed(stages):
+        scatter.reduce(hops)
+        if hops == min(2, p.nz - 1):
+            scatter.send_own_y()
+    result[...] = (
+        middle_v[...].astype(jnp.float32) + 0.5 * part[own].astype(jnp.float32)
+    ).astype(jnp.bfloat16)
+    with jax.named_scope("drain"):
+        for out in outs:
+            out.wait()
+        for move in moves:
+            move.drain()
+        gather.drain()
+        gather_next.drain()
+        scatter.drain()
+
+
+def both_halves(prompt, gains, weights, sizes):
     gr, fs, tp = sizes
     rows, columns = weights[0].shape
     count, depth = prompt.shape
@@ -748,25 +764,23 @@
     turned = turns(rows)
     across = (width, total) if turned else (total, width)
     piece = (width, rows) if turned else (rows, width)
-    served = jax.ShapeDtypeStruct(across, bf16)
     return pl.pallas_call(
-        functools.partial(first_kernel, sizes, count, rows_at_once, turned),
-        out_shape=[served] * 6
-        + [jax.ShapeDtypeStruct((count * fs, depth), bf16), jax.ShapeDtypeStruct((count, depth), bf16)],
+        functools.partial(main_kernel, sizes, count, rows_at_once, turned),
+        out_shape=[jax.ShapeDtypeStruct(across, bf16)] * 6 + [jax.ShapeDtypeStruct((count, depth), bf16)],
         in_specs=[ANY, VMEM, VMEM] + [ANY] * 6,
-        out_specs=[ANY] * 7 + [VMEM],
+        out_specs=[ANY] * 6 + [VMEM],
         scratch_shapes=[
             pltpu.VMEM((count, depth), bf16),
             pltpu.VMEM((6, rows, columns), jnp.float32),
             pltpu.VMEM((6, blocks, *piece), bf16),
-            pltpu.VMEM((3, *across), bf16),
+            pltpu.VMEM((6, *across), bf16),
             pltpu.VMEM((count * fs, depth), bf16),
             pltpu.VMEM((count * fs, depth), bf16),
             pltpu.VMEM((count * fs, depth), bf16),
             pltpu.VMEM((rows_at_once, width), bf16),
+            pltpu.VMEM((count, depth), bf16),
             pltpu.SemaphoreType.DMA((7,)),
-            pltpu.SemaphoreType.DMA((3,)),
-            pltpu.SemaphoreType.DMA,
+            pltpu.SemaphoreType.DMA((6,)),
             pltpu.SemaphoreType.DMA((2, fs, cuts_of(count), 4)),
             pltpu.SemaphoreType.DMA((2, fs, cuts_of(count))),
             *relayout_sems(6, blocks, sizes),
@@ -775,139 +789,41 @@
         compiler_params=pltpu.CompilerParams(
             collective_id=0, has_side_effects=True, vmem_limit_bytes=VMEM_LIMIT
         ),
-        name="first_half",
+        name="both_halves",
     )(prompt, *(gain.reshape(1, -1) for gain in gains), *weights)
 
 
-def second_kernel(fs, rows_at_once, turned, *refs):
-    (tokens, *served), refs = refs[:7], refs[7:]
-    (*outs, part), refs = refs[:7], refs[7:]
-    tokens_v, served_v, part_v, hidden, in_sem, out_sem, part_sem = refs
-    width = hidden.shape[1]
-    scales = scales_of(tokens.shape[1], width, fs)
-    loads = {m: pltpu.make_async_copy(served[m], served_v.at[m], in_sem.at[m]) for m in (0, 1, 2, 5)}
-    stores = [pltpu.make_async_copy(served_v.at[m], outs[m], out_sem.at[m]) for m in range(6)]
-
-    def load_slab(m, i, low, high):
-        slab = (pl.ds(low, high - low),) if turned else (slice(None), pl.ds(low, high - low))
-        return pltpu.make_async_copy(served[m].at[slab], served_v.at[(m, *slab)], in_sem.at[7 + 2 * i + m - 3])
-
-    slabs = slabs_of(width) if turned else [(0, width)]
-    load_tokens = pltpu.make_async_copy(tokens, tokens_v, in_sem.at[6])
-    load_tokens.start()
-    for i, (low, high) in enumerate(slabs):
-        for m in (3, 4):
-            load_slab(m, i, low, high).start()
-    for m in (5, 0, 1, 2):
-        loads[m].start()
-    load_tokens.wait()
-    tiles = tokens.shape[0] // rows_at_once
-
-    def tile(step, carry):
-        def ready(i):
-            @pl.when(step == 0)
-            def _():
-                if i is None:
-                    loads[5].wait()
-                elif i < len(slabs):
-                    for m in (3, 4):
-                        load_slab(m, i, *slabs[i]).wait()
-
-        start = pl.multiple_of(step * rows_at_once, rows_at_once)
-        weights = [served_v.at[m] for m in (3, 4, 5)]
-        ffn_rows(tokens_v, weights, part_v, hidden, start, scales, turned, ready)
-        rows = pl.ds(start, rows_at_once)
-        pltpu.make_async_copy(part_v.at[rows], part.at[rows], part_sem).start()
-
-        @pl.when(step == 0)
-        def _():
-            for m in range(3):
-                loads[m].wait()
-            for store in stores:
-                store.start()
-
-        return carry
-
-    lax.fori_loop(0, tiles, tile, 0)
-    wait_bytes(part_v, part_sem)
+def hand_over_kernel(parts, *refs):
+    sources, targets, (held, in_sem, out_sem) = refs[:6], refs[6:12], refs[12:]
+    height = held.shape[1] // parts
+    pieces = [(m, i, pl.ds(i * height, height)) for m in range(6) for i in range(parts)]
+    loads = [pltpu.make_async_copy(sources[m].at[rows], held.at[m, rows], in_sem.at[m, i]) for m, i, rows in pieces]
+    stores = [pltpu.make_async_copy(held.at[m, rows], targets[m].at[rows], out_sem.at[m, i]) for m, i, rows in pieces]
+    for load in loads:
+        load.start()
+    for load, store in zip(loads, stores):
+        load.wait()
+        store.start()
     for store in stores:
         store.wait()
 
 
-def second_half(tokens, served, fs, turned):
+def hand_over(served):
     across = served[0].shape
-    width = across[0 if turned else 1]
-    count, depth = tokens.shape
-    rows_at_once = count // 2
-    bf16 = jnp.bfloat16
+    parts = 2
     return pl.pallas_call(
-        functools.partial(second_kernel, fs, rows_at_once, turned),
-        out_shape=[jax.ShapeDtypeStruct(across, bf16)] * 6
-        + [jax.ShapeDtypeStruct((count, depth), bf16)],
-        in_specs=[ANY] * 7,
-        out_specs=[ANY] * 7,
+        functools.partial(hand_over_kernel, parts),
+        out_shape=[jax.ShapeDtypeStruct(across, jnp.bfloat16)] * 6,
+        in_specs=[ANY] * 6,
+        out_specs=[ANY] * 6,
         scratch_shapes=[
-            pltpu.VMEM((count, depth), bf16),
-            pltpu.VMEM((6, *across), bf16),
-            pltpu.VMEM((count, depth), bf16),
-            pltpu.VMEM((rows_at_once, width), bf16),
-            pltpu.SemaphoreType.DMA((7 + 2 * len(slabs_of(width)),)),
-            pltpu.SemaphoreType.DMA((6,)),
-            pltpu.SemaphoreType.DMA,
+            pltpu.VMEM((6, *across), jnp.bfloat16),
+            pltpu.SemaphoreType.DMA((6, parts)),
+            pltpu.SemaphoreType.DMA((6, parts)),
         ],
         compiler_params=pltpu.CompilerParams(vmem_limit_bytes=VMEM_LIMIT),
-        name="second_half",
-    )(tokens, *served)
-
-
-def last_kernel(sizes, count, partial, middle, result, part, part_sem, *scatter_refs):
-    p = Place(sizes)
-    scatter = Scatter(p, part, *scatter_refs[:3], scatter_refs[3:])
-
-    def load(z0):
-        rows = pl.ds(pl.multiple_of(z0 * p.ny * count, p.ny * count), p.ny * count)
-        return pltpu.make_async_copy(partial.at[rows], part.at[rows], part_sem.at[z0])
-
-    def begin(z0, sign):
-        load(z0).wait()
-        scatter.send_y(z0)
-
-    arrive = greet(neighbours(p))
-    for hops in range(p.nz - 1, -1, -1):
-        scatter.at_distance(hops, lambda z0, sign: load(z0).start())
-    arrive()
-    for hops in range(p.nz - 1, 0, -1):
-        scatter.at_distance(hops, begin)
-    load(p.z).wait()
-    for hops in range(p.nz - 1, -1, -1):
-        scatter.reduce(hops)
-        if hops == min(2, p.nz - 1):
-            scatter.send_own_y()
-    own = pl.ds(pl.multiple_of(p.f * count, count), count)
-    result[...] = (
-        middle[...].astype(jnp.float32) + 0.5 * part[own].astype(jnp.float32)
-    ).astype(jnp.bfloat16)
-    scatter.drain()
-
-
-def last_step(partial, middle, sizes):
-    fs = sizes[1]
-    count, depth = middle.shape
-    return pl.pallas_call(
-        functools.partial(last_kernel, sizes, count),
-        out_shape=jax.ShapeDtypeStruct((count, depth), jnp.bfloat16),
-        in_specs=[ANY, VMEM],
-        out_specs=VMEM,
-        scratch_shapes=[
-            pltpu.VMEM((fs * count, depth), jnp.bfloat16),
-            pltpu.SemaphoreType.DMA((fs // inner_of(fs),)),
-            *scatter_scratch(sizes, count, depth),
-        ],
-        compiler_params=pltpu.CompilerParams(
-            collective_id=1, has_side_effects=True, vmem_limit_bytes=VMEM_LIMIT
-        ),
-        name="last_step",
-    )(partial, middle)
+        name="hand_over",
+    )(*served)
 
 
 def on_device(
@@ -923,10 +839,9 @@
 ):
     sizes = tuple(lax.axis_size(axis) for axis in ("gr", "fs", "tp"))
     weights = (gate_first, up_first, down_first, gate_second, up_second, down_second)
-    *served, tokens, middle = first_half(prompt, (norm_first, norm_second), weights, sizes)
+    *served, result = both_halves(prompt, (norm_first, norm_second), weights, sizes)
+    served = hand_over(served)
     turned = turns(gate_first.shape[0])
-    *served, partial = second_half(tokens, served, sizes[1], turned)
-    result = last_step(partial, middle, sizes)
     if turned:
         served = [block.T for block in served]
     return (*served, result)

time: 246 us -> 233 us (0.947)
  Pallas kernels: 243 us -> 232 us
    pallas_call x3 -> x2, Pallas kernels: 243 us -> 232 us  [the longest x1 219 us: both_halves(): pl.pallas_call(functools.partial(main_kernel, sizes, count, rows_at_once,...]
where the time goes in v3:
time: 233 us
  Pallas kernels  232 us (100%)
    pallas_call x1, Pallas kernels, both_halves(): pl.pallas_call(functools.partial(main_kernel, sizes, count, rows_at_once,...  219 us
    pallas_call x1, Pallas kernels, hand_over(): pl.pallas_call(functools.partial(hand_over_kernel, parts), out_shape=[jax...  12.5 us

profile of v3, /device:TPU:0, one launch (start us, length us, event | category | flops | bytes accessed | tf_op | source)
XLA Modules:
  0.0 233.1 jit_solution(8897271482188959472)
XLA Ops:
  0.6 219.2 %both_halves.1 = (bf16[704,2048]{1,0:T(8,128)(2,1)}, bf16[704,2048]{1,0:T(8,128)(2,1)}, bf16[704,2048]{1,0:T(8,128)(2,1)}, bf16[704,2048]{1,0:T(8,128)(2,1)}, bf...) custom-call(bf16[96,2048]{1,0:T(8,128)(2,1)} %refs_0_.1, f32[1,128]{1,0:T(1,128)} %bitcast.8, ...), custom_call_target="tpu_custom_call" | custom-call | tf_op jit(solution)/shard_map/both_halves/pallas_call | solution.py:767
  219.9 0.0 copy-start
  219.9 12.5 %hand_over.1 = (bf16[704,2048]{1,0:T(8,128)(2,1)}, bf16[704,2048]{1,0:T(8,128)(2,1)}, bf16[704,2048]{1,0:T(8,128)(2,1)}, bf16[704,2048]{1,0:T(8,128)(2,1)}, bf16...) custom-call(bf16[704,2048]{1,0:T(8,128)(2,1)} %get-tuple-element.20.refs_0_, ...), custom_call_target="tpu_custom_call" | custom-call | tf_op jit(solution)/shard_map/hand_over/pallas_call | solution.py:814
  232.4 0.0 copy-done
  232.4 0.7 copy.17
Async XLA Ops:
  219.9 12.5 %copy-start = (bf16[96,2048]{1,0:T(8,128)(2,1)S(1)}, bf16[96,2048]{1,0:T(8,128)(2,1)}, u32[]{:S(2)}) copy-start(bf16[96,2048]{1,0:T(8,128)(2,1)} %get-tuple-element.46) | copy-start | bytes 1179652

commit v4 on v3

--- a/solution.py
+++ b/solution.py
@@ -9,7 +9,7 @@
 
 EPS = 1e-06
 MESH = pl.DeviceIdType.MESH
-VMEM_LIMIT = 63 * 1024 * 1024
+MAIN_VMEM_LIMIT = 42 * 1024 * 1024
 CUTS = 3
 SAME, NEAR, ACROSS = range(3)
 ANY = pl.BlockSpec(memory_space=pl.ANY)
@@ -614,8 +614,8 @@
 def main_kernel(sizes, count, rows_at_once, turned, *refs):
     (prompt, gain_first, gain_second, *weights), refs = refs[:9], refs[9:]
     (*served, result), refs = refs[:7], refs[7:]
-    (prompt_v, weights_v, pieces, served_v, tokens, tokens_next, part, hidden, middle_v), refs = refs[:9], refs[9:]
-    (in_sem, out_sem, ag_send, ag_recv, *refs) = refs
+    (prompt_v, weights_v, pieces, tokens, tokens_next, part, hidden, middle_v), refs = refs[:8], refs[8:]
+    (in_sem, ag_send, ag_recv, *refs) = refs
     relayout_refs, scatter_refs = refs[:6], refs[6:]
     p = Place(sizes)
     depth = tokens.shape[1]
@@ -628,7 +628,7 @@
             load.start()
 
     moves = [
-        Relayout(p, turned, pieces.at[m], served_v.at[m], [s.at[m] for s in relayout_refs])
+        Relayout(p, turned, pieces.at[m], served[m], [s.at[m] for s in relayout_refs])
         for m in range(6)
     ]
     gains = [gain_first, gain_first, None, gain_second, gain_second, None]
@@ -685,10 +685,6 @@
         moves[m].pass_far(ACROSS)
     for m in range(3):
         moves[m].wait_all_here()
-    outs = [pltpu.make_async_copy(served_v.at[m], served[m], out_sem.at[m]) for m in range(6)]
-    for m in range(3):
-        outs[m].start()
-
     scatter = Scatter(p, part, *scatter_refs[:3], scatter_refs[3:])
     tiles = p.fs * count // rows_at_once
     z_at_once = p.nz // tiles
@@ -697,7 +693,7 @@
         def tile(step, carry):
             at = jnp.where(2 * p.z < p.nz, tiles - 1 - step, step)
             start = pl.multiple_of(at * rows_at_once, rows_at_once)
-            weights = [served_v.at[first_weight + m] for m in range(3)]
+            weights = served[first_weight : first_weight + 3]
             ffn_rows(source, weights, part, hidden, start, scales, turned)
             scatter.send_y_of(lambda z0: z0 // z_at_once == at)
             return carry
@@ -731,8 +727,6 @@
     gather_next.run(p.nz)
     for m in range(3, 6):
         moves[m].wait_all_here()
-    for m in range(3, 6):
-        outs[m].start()
     scatter.drain()
     branch(tokens_next, 3)
     for hops in reversed(stages):
@@ -743,8 +737,6 @@
         middle_v[...].astype(jnp.float32) + 0.5 * part[own].astype(jnp.float32)
     ).astype(jnp.bfloat16)
     with jax.named_scope("drain"):
-        for out in outs:
-            out.wait()
         for move in moves:
             move.drain()
         gather.drain()
@@ -766,64 +758,51 @@
     piece = (width, rows) if turned else (rows, width)
     return pl.pallas_call(
         functools.partial(main_kernel, sizes, count, rows_at_once, turned),
-        out_shape=[jax.ShapeDtypeStruct(across, bf16)] * 6 + [jax.ShapeDtypeStruct((count, depth), bf16)],
+        out_shape=[pltpu.VMEM(across, bf16)] * 6 + [pltpu.VMEM((count, depth), bf16)],
         in_specs=[ANY, VMEM, VMEM] + [ANY] * 6,
-        out_specs=[ANY] * 6 + [VMEM],
+        out_specs=[VMEM] * 7,
         scratch_shapes=[
             pltpu.VMEM((count, depth), bf16),
             pltpu.VMEM((6, rows, columns), jnp.float32),
             pltpu.VMEM((6, blocks, *piece), bf16),
-            pltpu.VMEM((6, *across), bf16),
             pltpu.VMEM((count * fs, depth), bf16),
             pltpu.VMEM((count * fs, depth), bf16),
             pltpu.VMEM((count * fs, depth), bf16),
             pltpu.VMEM((rows_at_once, width), bf16),
             pltpu.VMEM((count, depth), bf16),
             pltpu.SemaphoreType.DMA((7,)),
-            pltpu.SemaphoreType.DMA((6,)),
             pltpu.SemaphoreType.DMA((2, fs, cuts_of(count), 4)),
             pltpu.SemaphoreType.DMA((2, fs, cuts_of(count))),
             *relayout_sems(6, blocks, sizes),
             *scatter_scratch(sizes, count, depth),
         ],
         compiler_params=pltpu.CompilerParams(
-            collective_id=0, has_side_effects=True, vmem_limit_bytes=VMEM_LIMIT
+            collective_id=0, has_side_effects=True, vmem_limit_bytes=MAIN_VMEM_LIMIT
         ),
         name="both_halves",
     )(prompt, *(gain.reshape(1, -1) for gain in gains), *weights)
 
 
-def hand_over_kernel(parts, *refs):
-    sources, targets, (held, in_sem, out_sem) = refs[:6], refs[6:12], refs[12:]
-    height = held.shape[1] // parts
-    pieces = [(m, i, pl.ds(i * height, height)) for m in range(6) for i in range(parts)]
-    loads = [pltpu.make_async_copy(sources[m].at[rows], held.at[m, rows], in_sem.at[m, i]) for m, i, rows in pieces]
-    stores = [pltpu.make_async_copy(held.at[m, rows], targets[m].at[rows], out_sem.at[m, i]) for m, i, rows in pieces]
-    for load in loads:
-        load.start()
-    for load, store in zip(loads, stores):
-        load.wait()
+def hand_over_kernel(*refs):
+    count = len(refs) // 2
+    sources, targets, sem = refs[:count], refs[count : 2 * count], refs[2 * count]
+    stores = [pltpu.make_async_copy(sources[m], targets[m], sem.at[m]) for m in range(count)]
+    for store in stores:
         store.start()
     for store in stores:
         store.wait()
 
 
-def hand_over(served):
-    across = served[0].shape
-    parts = 2
+def hand_over(results):
     return pl.pallas_call(
-        functools.partial(hand_over_kernel, parts),
-        out_shape=[jax.ShapeDtypeStruct(across, jnp.bfloat16)] * 6,
-        in_specs=[ANY] * 6,
-        out_specs=[ANY] * 6,
-        scratch_shapes=[
-            pltpu.VMEM((6, *across), jnp.bfloat16),
-            pltpu.SemaphoreType.DMA((6, parts)),
-            pltpu.SemaphoreType.DMA((6, parts)),
-        ],
-        compiler_params=pltpu.CompilerParams(vmem_limit_bytes=VMEM_LIMIT),
+        hand_over_kernel,
+        out_shape=[jax.ShapeDtypeStruct(block.shape, block.dtype) for block in results],
+        in_specs=[VMEM] * len(results),
+        out_specs=[ANY] * len(results),
+        scratch_shapes=[pltpu.SemaphoreType.DMA((len(results),))],
+        compiler_params=pltpu.CompilerParams(vmem_limit_bytes=4 * 1024 * 1024),
         name="hand_over",
-    )(*served)
+    )(*results)
 
 
 def on_device(
@@ -839,8 +818,8 @@
 ):
     sizes = tuple(lax.axis_size(axis) for axis in ("gr", "fs", "tp"))
     weights = (gate_first, up_first, down_first, gate_second, up_second, down_second)
-    *served, result = both_halves(prompt, (norm_first, norm_second), weights, sizes)
-    served = hand_over(served)
+    results = both_halves(prompt, (norm_first, norm_second), weights, sizes)
+    *served, result = hand_over(results)
     turned = turns(gate_first.shape[0])
     if turned:
         served = [block.T for block in served]

time: 233 us -> 226 us (0.970)
  Pallas kernels: 232 us -> 225 us
    pallas_call x1, Pallas kernels: 12.5 us -> 6.18 us  [hand_over(): pl.pallas_call(hand_over_kernel, out_shape=[jax.ShapeDtypeStruct(block.sh...]
where the time goes in v4:
time: 226 us
  Pallas kernels  225 us (100%)
    pallas_call x1, Pallas kernels, both_halves(): pl.pallas_call(functools.partial(main_kernel, sizes, count, rows_at_once,...  219 us
    pallas_call x1, Pallas kernels, hand_over(): pl.pallas_call(hand_over_kernel, out_shape=[jax.ShapeDtypeStruct(block.sh...  6.18 us

profile of v4, /device:TPU:0, one launch (start us, length us, event | category | flops | bytes accessed | tf_op | source)
XLA Modules:
  0.0 225.6 jit_solution(6790242344807583249)
XLA Ops:
  0.6 218.6 %both_halves.1 = (bf16[704,2048]{1,0:T(8,128)(2,1)S(1)}, bf16[704,2048]{1,0:T(8,128)(2,1)S(1)}, bf16[704,2048]{1,0:T(8,128)(2,1)S(1)}, bf16[704,2048]{1,0:T(8,12...) custom-call(bf16[96,2048]{1,0:T(8,128)(2,1)} %refs_0_.1, ...), custom_call_target="tpu_custom_call" | custom-call | tf_op jit(solution)/shard_map/both_halves/pallas_call | solution.py:759
  219.3 6.2 %hand_over.1 = (bf16[704,2048]{1,0:T(8,128)(2,1)}, bf16[704,2048]{1,0:T(8,128)(2,1)}, bf16[704,2048]{1,0:T(8,128)(2,1)}, bf16[704,2048]{1,0:T(8,128)(2,1)}, bf16...) custom-call(bf16[704,2048]{1,0:T(8,128)(2,1)S(1)} %get-tuple-element.21.refs_0_, ...), custom_call_target="tpu_custom_call" | custom-call | tf_op jit(solution)/shard_map/hand_over/pallas_call | solution.py:797

commit v5 on v4

--- a/solution.py
+++ b/solution.py
@@ -591,7 +591,7 @@
         act = gate_pre / (1.0 + jnp.exp(-gate_pre)) * up_pre
         hidden[:, low:high] = act.astype(jnp.bfloat16)
     ready(None)
-    chunk = 256 if depth % 256 == 0 else depth
+    chunk = 512 if depth % 512 == 0 else depth
 
     def body(i, carry):
         low = pl.multiple_of(i * chunk, chunk)

time: 226 us -> 224 us (level)
  no operation moved by 1% of the time
where the time goes in v5:
time: 224 us
  Pallas kernels  223 us (100%)
    pallas_call x1, Pallas kernels, both_halves(): pl.pallas_call(functools.partial(main_kernel, sizes, count, rows_at_once,...  217 us
    pallas_call x1, Pallas kernels, hand_over(): pl.pallas_call(hand_over_kernel, out_shape=[jax.ShapeDtypeStruct(block.sh...  6.18 us

profile of v5, /device:TPU:0, one launch (start us, length us, event | category | flops | bytes accessed | tf_op | source)
XLA Modules:
  0.0 223.8 jit_solution(12562468804801411374)
XLA Ops:
  0.6 216.8 %both_halves.1 = (bf16[704,2048]{1,0:T(8,128)(2,1)S(1)}, bf16[704,2048]{1,0:T(8,128)(2,1)S(1)}, bf16[704,2048]{1,0:T(8,128)(2,1)S(1)}, bf16[704,2048]{1,0:T(8,12...) custom-call(bf16[96,2048]{1,0:T(8,128)(2,1)} %refs_0_.1, ...), custom_call_target="tpu_custom_call" | custom-call | tf_op jit(solution)/shard_map/both_halves/pallas_call | solution.py:759
  217.5 6.2 %hand_over.1 = (bf16[704,2048]{1,0:T(8,128)(2,1)}, bf16[704,2048]{1,0:T(8,128)(2,1)}, bf16[704,2048]{1,0:T(8,128)(2,1)}, bf16[704,2048]{1,0:T(8,128)(2,1)}, bf16...) custom-call(bf16[704,2048]{1,0:T(8,128)(2,1)S(1)} %get-tuple-element.21.refs_0_, ...), custom_call_target="tpu_custom_call" | custom-call | tf_op jit(solution)/shard_map/hand_over/pallas_call | solution.py:797
